TPU v7x, 256 devices: a whole 4x4x8 slice. The times are simulated.
256 devices in a mesh: sp: 64 (over z, x, core), tp: 4 (over y).
Axes of the slice: x: 4, y: 4, z: 8, core: 2. Of those that a mesh axis runs over, the one named last changes fastest.
Arguments:
- stream: bfloat16 [32768, 2048], P(('sp', 'tp')), may hold values from -6 to 6
- pool_in: bfloat16 [32768, 1024], P('sp', 'tp'), may hold values from -6 to 6
- doc_ids: int32 [32768], P('sp'), may hold values from 0 to 7, never falling along the last dimension, each value on 1 to 8192 neighbouring positions
- pool_map: bfloat16 [4, 256, 512], P('tp'), may hold values from -0.375 to 0.375
- pool_scale: float32 [2048], P('tp'), may hold values from 0.1 to 1.9
- out_weight: bfloat16 [2048, 2048], P('tp'), may hold values from -0.125 to 0.125
- norm_gain: float32 [2048], replicated, may hold values from 0.1 to 1.9
- routes: int32 [32768, 2], P('sp'), may hold values from 0 to 63, all different within a row; in each aligned block of 128 rows (0 to 127, 128 to 255, ...) at most 6 rows name the same one
- route_weight: float32 [32768, 2], P(('sp', 'tp')), may hold values from 0.2 to 1
- expert_gate: bfloat16 [64, 2048, 1024], P('sp', None, 'tp'), may hold values from -0.125 to 0.125
- expert_up: bfloat16 [64, 2048, 1024], P('sp', None, 'tp'), may hold values from -0.125 to 0.125
- expert_down: bfloat16 [64, 1024, 2048], P('sp', 'tp'), may hold values from -0.1875 to 0.1875
Outputs:
- result: bfloat16 [32768, 2048], P(('sp', 'tp'))
Inputs may be any that keep to these rules, and one draw needn't show every extreme that they name: `routes`: each token names 2 different experts; in each aligned block of 128 rows no expert is named by more than 6 rows, a bound that some block reaches. `doc_ids`: never falling; each document holds at most 8192 positions.
All inputs are finite; a program needn't handle non-finite values.
Results may differ from a plain program's by a relative error of at most 0.014.
Values may be sent and summed in bfloat16 or wider, within the bound.
A program may use at most 64 MiB of HBM per device.

v0:
```python
import jax
import jax.numpy as jnp
from jax import lax
from jax.sharding import PartitionSpec as P

SPAN = 16


EPS = 1e-06


def passed_along(value, axis, by):
    length = lax.axis_size(axis)
    pairs = [(i, i + by) for i in range(length) if 0 <= i + by < length]
    return lax.ppermute(value, axis, pairs)


def cut_along(value, dim, length):
    before, after = (value.shape[:dim], value.shape[dim + 1 :])
    return jnp.moveaxis(value.reshape(*before, length, -1, *after), dim, 0)


def sum_at_owner(value, axis, dim):
    length = lax.axis_size(axis)
    tiles = lax.all_to_all(cut_along(value, dim, length), axis, 0, 0, tiled=True)
    return jnp.sum(tiles.astype(jnp.float32), axis=0)


def slot_table(route_block, expert_count, capacity, top_count):
    flattened = route_block.reshape(-1)
    one_hot = (flattened[:, None] == jnp.arange(expert_count, dtype=jnp.int32)[None, :]).astype(
        jnp.int32
    )
    ranking = jnp.sum((jnp.cumsum(one_hot, axis=0) - one_hot) * one_hot, axis=1)
    target_slot = flattened * capacity + ranking
    matches = target_slot[None, :] == jnp.arange(expert_count * capacity, dtype=jnp.int32)[:, None]
    sources = jnp.sum(
        jnp.where(matches, jnp.arange(flattened.shape[0], dtype=jnp.int32)[None, :], 0), axis=1
    )
    filled = jnp.any(matches, axis=1)
    return (target_slot, sources // top_count, filled)


def per_device(
    stream,
    pool_in,
    doc_ids,
    pool_map,
    pool_scale,
    out_weight,
    norm_gain,
    routes,
    route_weight,
    expert_gate,
    expert_up,
    expert_down,
):
    row_count = pool_in.shape[0]
    model_width = stream.shape[1]
    top_count = routes.shape[1]
    tp_count = lax.axis_size("tp")
    expert_count = lax.axis_size("sp")
    quarter = row_count // tp_count
    capacity = max(2, 3 * top_count * quarter // (2 * expert_count))
    reach_rows = SPAN - 1
    tail_rows = (
        pool_in[row_count - reach_rows :],
        doc_ids[row_count - reach_rows :].astype(jnp.bfloat16),
    )
    prior_rows, prior_docs = passed_along((tail_rows[0], tail_rows[1]), "sp", 1)
    extended = jnp.concatenate([prior_rows, pool_in], axis=0).astype(jnp.float32)
    extended_docs = jnp.concatenate([prior_docs.astype(jnp.float32), doc_ids.astype(jnp.float32)])
    own_docs = doc_ids.astype(jnp.float32)
    window = jnp.left_shift(jnp.int32(2), lax.axis_index("tp"))
    positions = lax.axis_index("sp") * row_count + jnp.arange(row_count, dtype=jnp.int32)
    running = jnp.zeros(pool_in.shape, jnp.float32)
    counts = jnp.zeros((row_count,), jnp.float32)
    for offset in range(reach_rows + 1):
        begin_row = reach_rows - offset
        piece_rows = extended[begin_row : begin_row + row_count]
        piece_docs = extended_docs[begin_row : begin_row + row_count]
        in_window = (offset < window) & (positions - offset >= 0) & (piece_docs == own_docs)
        running = running + jnp.where(in_window[:, None], piece_rows, 0.0)
        counts = counts + in_window.astype(jnp.float32)
    pooled = (running / counts[:, None] - pool_in.astype(jnp.float32)).astype(jnp.bfloat16)
    branch = (jnp.dot(pooled, pool_map[0], preferred_element_type=jnp.float32) * pool_scale).astype(
        jnp.bfloat16
    )
    projected = sum_at_owner(
        jnp.dot(branch, out_weight, preferred_element_type=jnp.float32).astype(jnp.bfloat16),
        "tp",
        0,
    )
    mixed_rows = (stream.astype(jnp.float32) + projected).astype(jnp.bfloat16)
    mixed_up = mixed_rows.astype(jnp.float32)
    normed = (
        mixed_up * lax.rsqrt(jnp.mean(mixed_up * mixed_up, axis=1, keepdims=True) + EPS) * norm_gain
    ).astype(jnp.bfloat16)
    own_routes = lax.dynamic_slice_in_dim(routes, lax.axis_index("tp") * quarter, quarter, 0)
    own_slots, own_sources, own_filled = slot_table(own_routes, expert_count, capacity, top_count)
    token_index = own_sources.reshape(expert_count, 1, capacity)
    filled_slots = own_filled.reshape(expert_count, 1, capacity)
    dispatch = jnp.where(filled_slots[..., None], normed[token_index], jnp.zeros((), jnp.bfloat16))
    arrived = lax.all_to_all(dispatch, "sp", split_axis=0, concat_axis=0, tiled=True)
    arrived = lax.all_gather(arrived, "tp", axis=1, tiled=True)
    stacked = arrived.reshape(-1, model_width)
    gate_pre = jnp.dot(stacked, expert_gate[0], preferred_element_type=jnp.float32)
    up_pre = jnp.dot(stacked, expert_up[0], preferred_element_type=jnp.float32)
    hidden = (jax.nn.silu(gate_pre) * up_pre).astype(jnp.bfloat16)
    partial_out = jnp.dot(hidden, expert_down[0], preferred_element_type=jnp.float32).reshape(
        arrived.shape
    )
    summed = sum_at_owner(partial_out.astype(jnp.bfloat16), "tp", 1).astype(jnp.bfloat16)
    returned = lax.all_to_all(summed, "sp", split_axis=0, concat_axis=0, tiled=True)
    outputs = returned.reshape(expert_count * capacity, model_width)
    picked = outputs[own_slots].astype(jnp.float32).reshape(quarter, top_count, model_width)
    combined = jnp.sum(route_weight[:, :, None] * picked, axis=1)
    return (mixed_up + combined).astype(jnp.bfloat16)


def solution(mesh):
    in_specs = (
        P(("sp", "tp"), None),
        P("sp", "tp"),
        P("sp"),
        P("tp", None, None),
        P("tp"),
        P("tp", None),
        P(),
        P("sp", None),
        P(("sp", "tp"), None),
        P("sp", None, "tp"),
        P("sp", None, "tp"),
        P("sp", "tp", None),
    )
    out_specs = P(("sp", "tp"), None)
    return jax.shard_map(
        per_device, mesh=mesh, in_specs=in_specs, out_specs=out_specs, check_vma=False
    )
```

profile of v0, /device:TPU:1, one launch (start us, length us, event | category | flops | bytes accessed | tf_op | source)
XLA Modules:
  0.0 377.9 jit_solution(2949899418363238842)
XLA Ops:
  6.5 0.0 copy-start
  6.5 0.9 fusion.128
  7.4 0.1 slice.108
  7.5 4.5 %collective-permute-start.1 = (bf16[15]{0:T(256)(128)(2,1)S(1)}, bf16[15]{0:T(256)(128)(2,1)S(1)}, u32[]{:S(2)}, u32[]{:S(2)}) collective-permute-start(bf16[15]{0:T(256)(128)(2,1)S(1)} %slice.108), channel_id=1, source_target_pairs={{0,4},{4,8},{8,12},{12,16},{16,20},{20,24},{24,28},{28,32},{32,36}... | collective-permute-start | bytes 98 | tf_op jit(solution)/shard_map/ppermute | solution.py:15
  12.0 0.7 slice.106
  12.7 1.9 collective-permute-start
  14.6 0.0 collective-permute-done.1
  14.6 0.1 pad_maximum_fusion
  14.7 0.8 convert_add_fusion.1
  15.5 0.2 collective-permute-done
  15.7 1.0 maximum_convert_fusion
  16.7 0.0 copy-done
  16.7 5.4 %convolution_convert_fusion = bf16[512,2048]{1,0:T(8,128)(2,1)} fusion(bf16[512,2048]{1,0:T(8,128)(2,1)S(1)} %copy-done, f32[512]{0:T(512)} %param.16, bf16[512,256]{1,0:T(8,128)(2,1)} %param.13, f32[527,256]{1,0:T(8,128)S(1)} %maximum_convert_fusion, bf16[1,256,512]{2,1,0:T(8,128)(2,1)} %param.15, f32[512]{0:T(512)S(1)} %get-tuple-element.9, ...), kind=kOutput, calls=%fused_computation.5 | convolution fusion | flops 1214119936 | bytes 13119488 | tf_op jit(solution)/shard_map/dot_general | solution.py:90
  22.1 4.2 %all-to-all-start = ((bf16[4,128,2048]{2,1,0:T(8,128)(2,1)}), bf16[4,128,2048]{2,1,0:T(8,128)(2,1)S(1)}, u32[]{:S(2)}, u32[]{:S(2)}) async-start(bf16[4,128,2048]{2,1,0:T(8,128)(2,1)} %bitcast.58), calls=%async_computation | async-start | bytes 4194304 | tf_op jit(solution)/shard_map/all_to_all | solution.py:25
  26.3 0.7 broadcast_multiply_fusion
  27.1 0.1 copy.35
  27.2 0.1 eq.103
  27.3 0.1 reshape.209
  27.5 0.6 reduce-window.6
  28.1 0.2 slice_reduce_fusion
  28.3 0.1 fusion.73
  28.4 0.2 select_reduce_fusion
  28.6 0.1 reduce_sum.67
  28.8 0.1 reshape.217
  28.9 0.2 fusion.30
  29.1 0.2 broadcast_in_dim.172
  29.2 0.0 copy-start.5
  29.2 22.9 %all-to-all-done = bf16[4,128,2048]{2,1,0:T(8,128)(2,1)S(1)} async-done(((bf16[4,128,2048]{2,1,0:T(8,128)(2,1)}), bf16[4,128,2048]{2,1,0:T(8,128)(2,1)S(1)}, u32[]{:S(2)}, u32[]{:S(2)}) %all-to-all-start) | async-done | bytes 2097184 | tf_op jit(solution)/shard_map/all_to_all | solution.py:25
  52.2 0.4 convert_reduce_fusion
  52.6 0.3 fusion.2
  52.8 0.0 copy-done.5
  52.8 0.2 fusion.4
  53.0 2.5 gather_fusion
  55.5 1.6 reshape.216
  57.1 1.8 select_bitcast_fusion
  59.0 62.1 %all_to_all.20 = bf16[64,1,6,2048]{3,2,1,0:T(8,128)(2,1)S(1)} all-to-all(bf16[64,1,6,2048]{3,2,1,0:T(8,128)(2,1)S(1)} %select_bitcast_fusion), channel_id=1, replica_groups=mesh['sp'=64,'tp'=4] {'sp'}, dimensions={0} | all-to-all | bytes 3145728 | tf_op jit(solution)/shard_map/all_to_all | solution.py:104
  121.1 2.0 copy.39
  123.1 0.0 all-gather.2.cloned.1.call-update
  123.1 64.0 %all-gather.2.cloned.1.call-done = bf16[64,4,6,2048]{3,0,2,1:T(8,128)(2,1)} async-done(((bf16[64,1,6,2048]{3,0,2,1:T(8,128)(2,1)}), bf16[64,4,6,2048]{3,0,2,1:T(8,128)(2,1)}) %all-gather.2.cloned.1.call-update) | async-done | bytes 6291472 | tf_op jit(solution)/shard_map/all_gather | solution.py:105
  187.1 9.6 %copy.40 = bf16[64,4,6,2048]{3,2,1,0:T(8,128)(2,1)} copy(bf16[64,4,6,2048]{3,0,2,1:T(8,128)(2,1)} %all-gather.2.cloned.1.call-done) | data formatting | bytes 12582912 | tf_op jit(solution)/shard_map/all_gather | solution.py:105
  196.7 11.1 %reshape.211 = bf16[1536,2048]{1,0:T(8,128)(2,1)} reshape(bf16[64,4,6,2048]{3,2,1,0:T(8,128)(2,1)} %copy.40) | data formatting | bytes 12582912 | tf_op jit(solution)/shard_map/reshape | solution.py:106
  207.9 0.0 copy-done.7
  207.9 4.8 %fusion.8 = f32[1536,256]{1,0:T(8,128)S(1)} fusion(bf16[1536,2048]{1,0:T(8,128)(2,1)} %reshape.211, bf16[1,2048,256]{2,1,0:T(8,128)(2,1)S(1)} %copy-done.7), kind=kOutput, calls=%fused_computation.21 | convolution fusion | flops 1610612736 | bytes 8912896 | tf_op jit(solution)/shard_map/dot_general | solution.py:107
  212.7 0.0 copy-done.2
  212.7 0.0 copy-done.8
  212.7 2.1 fusion
  214.8 0.0 copy-start.3
  214.8 0.3 dot_general.21
  215.1 0.9 copy-done.3
  216.0 2.0 convert_bitcast_fusion
  218.0 73.4 %all_to_all.21 = bf16[4,64,1,6,2048]{4,1,3,2,0:T(8,128)(2,1)S(1)} all-to-all(bf16[4,64,1,6,2048]{4,1,3,2,0:T(8,128)(2,1)S(1)} %convert_bitcast_fusion), channel_id=1, replica_groups=mesh['sp'=64,'tp'=4] {'tp'}, dimensions={0} | all-to-all | bytes 12582912 | tf_op jit(solution)/shard_map/all_to_all | solution.py:25
  291.5 1.2 bitcast_reduce_fusion
  292.7 2.2 copy.44
  294.9 12.3 %all-to-all-start.3 = ((bf16[64,1,6,2048]{3,2,1,0:T(8,128)(2,1)}), bf16[64,1,6,2048]{3,2,1,0:T(8,128)(2,1)}, u32[]{:S(2)}, u32[]{:S(2)}) async-start(bf16[64,1,6,2048]{3,2,1,0:T(8,128)(2,1)} %copy.44), calls=%async_computation.3 | async-start | bytes 4194304 | tf_op jit(solution)/shard_map/all_to_all | solution.py:114
  307.2 0.1 copy.45
  307.3 0.1 mul.92
  307.5 0.1 copy.34
  307.6 49.2 %all-to-all-done.3 = bf16[64,1,6,2048]{3,2,1,0:T(8,128)(2,1)} async-done(((bf16[64,1,6,2048]{3,2,1,0:T(8,128)(2,1)}), bf16[64,1,6,2048]{3,2,1,0:T(8,128)(2,1)}, u32[]{:S(2)}, u32[]{:S(2)}) %all-to-all-start.3) | async-done | bytes 1572896 | tf_op jit(solution)/shard_map/all_to_all | solution.py:114
  356.8 2.6 reshape.213
  359.4 2.3 gather_fusion.1
  361.8 3.5 reshape.214
  365.3 4.8 %multiply_reduce_fusion = f32[128,2048]{1,0:T(8,128)S(1)} fusion(f32[128,2,2048]{2,1,0:T(2,128)} %reshape.214, f32[128,2]{1,0:T(8,128)S(1)} %copy.34), kind=kLoop, calls=%fused_computation.8 | loop fusion | flops 786432 | bytes 3146752 | tf_op jit(solution)/shard_map/reduce_sum | solution.py:117
  370.1 0.9 fusion.5
  371.1 0.0 copy-done.1
  (19 shorter events, 0.1 us)
Async XLA Ops:
  6.5 10.2 %copy-start = (bf16[512,2048]{1,0:T(8,128)(2,1)S(1)}, bf16[512,2048]{1,0:T(8,128)(2,1)}, u32[]{:S(2)}) copy-start(bf16[512,2048]{1,0:T(8,128)(2,1)} %param.17) | copy-start | bytes 6291460
  7.5 7.2 %collective-permute-start.1 = (bf16[15]{0:T(256)(128)(2,1)S(1)}, bf16[15]{0:T(256)(128)(2,1)S(1)}, u32[]{:S(2)}, u32[]{:S(2)}) collective-permute-start(bf16[15]{0:T(256)(128)(2,1)S(1)} %slice.108), channel_id=1, source_target_pairs={{0,4},{4,8},{8,12},{12,16},{16,20},{20,24},{24,28},{28,32},{32,36}... | collective-permute-start | bytes 98 | tf_op jit(solution)/shard_map/ppermute | solution.py:15
  12.7 3.1 collective-permute-start
  22.1 30.0 %all-to-all-start = ((bf16[4,128,2048]{2,1,0:T(8,128)(2,1)}), bf16[4,128,2048]{2,1,0:T(8,128)(2,1)S(1)}, u32[]{:S(2)}, u32[]{:S(2)}) async-start(bf16[4,128,2048]{2,1,0:T(8,128)(2,1)} %bitcast.58), calls=%async_computation | async-start | bytes 4194304 | tf_op jit(solution)/shard_map/all_to_all | solution.py:25
  26.3 26.2 %copy-start.4 = (bf16[128,2048]{1,0:T(8,128)(2,1)S(1)}, bf16[128,2048]{1,0:T(8,128)(2,1)}, u32[]{:S(2)}) copy-start(bf16[128,2048]{1,0:T(8,128)(2,1)} %param.12) | copy-start | bytes 1572868
  26.3 160.8 %all-gather.2.cloned.1.call-start = ((), (), s32[]{:S(2)}) async-start(), calls=%async_computation.4 | async-start | bytes 7864320 | tf_op jit(solution)/shard_map/all_gather | solution.py:105
  29.2 23.6 %copy-start.5 = (f32[2048]{0:T(1024)S(1)}, f32[2048]{0:T(1024)}, u32[]{:S(2)}) copy-start(f32[2048]{0:T(1024)} %param.18) | copy-start | bytes 24580
  196.7 11.1 %copy-start.7 = (bf16[1,2048,256]{2,1,0:T(8,128)(2,1)S(1)}, bf16[1,2048,256]{2,1,0:T(8,128)(2,1)}, u32[]{:S(2)}) copy-start(bf16[1,2048,256]{2,1,0:T(8,128)(2,1)} %param.21) | copy-start | bytes 3145732
  207.9 4.8 %copy-start.2 = (bf16[1536,2048]{1,0:T(8,128)(2,1)S(1)}, bf16[1536,2048]{1,0:T(8,128)(2,1)}, u32[]{:S(2)}) copy-start(bf16[1536,2048]{1,0:T(8,128)(2,1)} %reshape.211) | copy-start | bytes 18874372
  207.9 4.9 %copy-start.8 = (bf16[1,2048,256]{2,1,0:T(8,128)(2,1)S(1)}, bf16[1,2048,256]{2,1,0:T(8,128)(2,1)}, u32[]{:S(2)}) copy-start(bf16[1,2048,256]{2,1,0:T(8,128)(2,1)} %param.22) | copy-start | bytes 3145732
  214.8 1.2 copy-start.3
  294.9 12.5 %copy-start.6 = (f32[128,2]{0,1:T(2,128)S(1)}, f32[128,2]{0,1:T(2,128)}, u32[]{:S(2)}) copy-start(f32[128,2]{0,1:T(2,128)} %param.20) | copy-start | bytes 3076
  294.9 61.9 %all-to-all-start.3 = ((bf16[64,1,6,2048]{3,2,1,0:T(8,128)(2,1)}), bf16[64,1,6,2048]{3,2,1,0:T(8,128)(2,1)}, u32[]{:S(2)}, u32[]{:S(2)}) async-start(bf16[64,1,6,2048]{3,2,1,0:T(8,128)(2,1)} %copy.44), calls=%async_computation.3 | async-start | bytes 4194304 | tf_op jit(solution)/shard_map/all_to_all | solution.py:114
  361.8 9.3 %copy-start.1 = (bf16[512,2048]{1,0:T(8,128)(2,1)S(1)}, bf16[512,2048]{1,0:T(8,128)(2,1)}, u32[]{:S(2)}) copy-start(bf16[512,2048]{1,0:T(8,128)(2,1)} %param.17) | copy-start | bytes 6291460
Sparse Core Ops, SparseCore 0:
  123.3 63.7 all-gather.1
where the time goes:
time: 379 us; the launch traced here: 378 us
  waiting for transfers between devices  136 us (36%)
  blocking collectives  136 us (36%)
  local copies, waits for them, and re-layouts  40.9 us (11%)
  starting transfers between devices  22.9 us (6%)
  matrix products  14.3 us (4%)
  other arithmetic  14.2 us (4%)
  between operations  13.7 us (4%)
    all_to_all x1, blocking collectives, sum_at_owner(): lax.all_to_all(cut_along(value, dim, length), axis, 0, 0, tiled=True)  73.4 us
    all_gather x1, waiting for transfers between devices, per_device(): arrived = lax.all_gather(arrived, 'tp', axis=1, tiled=True)  64 us
    all_to_all x1, blocking collectives, per_device(): lax.all_to_all(dispatch, 'sp', split_axis=0, concat_axis=0, tiled=True)  62.1 us
    all_to_all x1, waiting for transfers between devices, per_device(): lax.all_to_all(summed, 'sp', split_axis=0, concat_axis=0, tiled=True)  49.2 us
    all_to_all x1, waiting for transfers between devices, sum_at_owner(): lax.all_to_all(cut_along(value, dim, length), axis, 0, 0, tiled=True)  22.9 us
    all_to_all x1, starting transfers between devices, per_device(): lax.all_to_all(summed, 'sp', split_axis=0, concat_axis=0, tiled=True)  12.3 us
    reshape x1, local copies, waits for them, and re-layouts, per_device(): stacked = arrived.reshape(-1, model_width)  11.1 us
    all_gather x1, local copies, waits for them, and re-layouts, per_device(): arrived = lax.all_gather(arrived, 'tp', axis=1, tiled=True)  9.61 us
  transfers between devices with their start and end apart: 5, of which 4 were waited for; matrix products, arithmetic and copies ran while one was open for 1% of the time, Pallas kernels for 0%

commit v1 on v0

--- a/solution.py
+++ b/solution.py
@@ -62,6 +62,9 @@
     expert_count = lax.axis_size("sp")
     quarter = row_count // tp_count
     capacity = max(2, 3 * top_count * quarter // (2 * expert_count))
+    all_gate = lax.all_gather(expert_gate, "tp", axis=0, tiled=True)
+    all_up = lax.all_gather(expert_up, "tp", axis=0, tiled=True)
+    all_down = lax.all_gather(expert_down, "tp", axis=0, tiled=True)
     reach_rows = SPAN - 1
     tail_rows = (
         pool_in[row_count - reach_rows :],
@@ -102,15 +105,15 @@
     filled_slots = own_filled.reshape(expert_count, 1, capacity)
     dispatch = jnp.where(filled_slots[..., None], normed[token_index], jnp.zeros((), jnp.bfloat16))
     arrived = lax.all_to_all(dispatch, "sp", split_axis=0, concat_axis=0, tiled=True)
-    arrived = lax.all_gather(arrived, "tp", axis=1, tiled=True)
     stacked = arrived.reshape(-1, model_width)
-    gate_pre = jnp.dot(stacked, expert_gate[0], preferred_element_type=jnp.float32)
-    up_pre = jnp.dot(stacked, expert_up[0], preferred_element_type=jnp.float32)
-    hidden = (jax.nn.silu(gate_pre) * up_pre).astype(jnp.bfloat16)
-    partial_out = jnp.dot(hidden, expert_down[0], preferred_element_type=jnp.float32).reshape(
-        arrived.shape
-    )
-    summed = sum_at_owner(partial_out.astype(jnp.bfloat16), "tp", 1).astype(jnp.bfloat16)
+    expert_sum = jnp.zeros(stacked.shape, jnp.float32)
+    for part in range(tp_count):
+        gate_pre = jnp.dot(stacked, all_gate[part], preferred_element_type=jnp.float32)
+        up_pre = jnp.dot(stacked, all_up[part], preferred_element_type=jnp.float32)
+        hidden = (jax.nn.silu(gate_pre) * up_pre).astype(jnp.bfloat16)
+        part_out = jnp.dot(hidden, all_down[part], preferred_element_type=jnp.float32)
+        expert_sum = expert_sum + part_out.astype(jnp.bfloat16).astype(jnp.float32)
+    summed = expert_sum.astype(jnp.bfloat16).reshape(arrived.shape)
     returned = lax.all_to_all(summed, "sp", split_axis=0, concat_axis=0, tiled=True)
     outputs = returned.reshape(expert_count * capacity, model_width)
     picked = outputs[own_slots].astype(jnp.float32).reshape(quarter, top_count, model_width)

time: 379 us -> 304 us (0.80)
  blocking collectives: 136 us -> 64.7 us
  matrix products: 14.3 us -> 34.3 us
  local copies, waits for them, and re-layouts: 40.9 us -> 27.7 us
  waiting for transfers between devices: 136 us -> 127 us
    all_to_all x1 -> x0, blocking collectives: 73.4 us -> none  [sum_at_owner(): lax.all_to_all(cut_along(value, dim, length), axis, 0, 0, tiled=True)]
    all_gather x1 -> x3, waiting for transfers between devices: 64 us -> 31.1 us  [the longest x1 31 us: per_device(): all_down = lax.all_gather(expert_down, 'tp', axis=0, tiled=True)]
    dot_general x3 -> x8, matrix products: 8.89 us -> 29.9 us  [the longest x4 21.8 us: per_device(): jnp.dot(hidden, all_down[part], preferred_element_type=jnp.float32)]
    all_to_all x1, waiting for transfers between devices: 22.9 us -> 43.3 us  [sum_at_owner(): lax.all_to_all(cut_along(value, dim, length), axis, 0, 0, tiled=True)]
    all_gather x1 -> x0, local copies, waits for them, and re-layouts: 9.61 us -> none  [per_device(): arrived = lax.all_gather(arrived, 'tp', axis=1, tiled=True)]
    reshape x1, local copies, waits for them, and re-layouts: 11.1 us -> 3.7 us  [per_device(): stacked = arrived.reshape(-1, model_width)]
  transfers between devices with their start and end apart: 5 -> 7, of which waited for: 4 -> 4; matrix products, arithmetic and copies ran while one was open for 1% -> 11% of each run, Pallas kernels for 0% -> 0%
where the time goes in v1:
time: 304 us; the launch traced here: 302 us
  waiting for transfers between devices  127 us (42%)
  blocking collectives  64.7 us (21%)
  matrix products  34.3 us (11%)
  local copies, waits for them, and re-layouts  27.7 us (9%)
  starting transfers between devices  22.2 us (7%)
  between operations  13.4 us (4%)
  other arithmetic  13.2 us (4%)
    all_to_all x1, blocking collectives, per_device(): lax.all_to_all(dispatch, 'sp', split_axis=0, concat_axis=0, tiled=True)  64.7 us
    all_to_all x1, waiting for transfers between devices, per_device(): lax.all_to_all(summed, 'sp', split_axis=0, concat_axis=0, tiled=True)  49.2 us
    all_to_all x1, waiting for transfers between devices, sum_at_owner(): lax.all_to_all(cut_along(value, dim, length), axis, 0, 0, tiled=True)  43.3 us
    all_gather x1, waiting for transfers between devices, per_device(): all_down = lax.all_gather(expert_down, 'tp', axis=0, tiled=True)  31 us
    dot_general x4, matrix products, per_device(): jnp.dot(hidden, all_down[part], preferred_element_type=jnp.float32)  21.8 us
    all_to_all x1, starting transfers between devices, per_device(): lax.all_to_all(summed, 'sp', split_axis=0, concat_axis=0, tiled=True)  11.2 us
    dot_general x4, matrix products, per_device(): jnp.dot(stacked, all_gate[part], preferred_element_type=jnp.float32)  8.1 us
    gather x2, local copies, waits for them, and re-layouts, per_device(): normed[token_index]  6.78 us
  transfers between devices with their start and end apart: 7, of which 4 were waited for; matrix products, arithmetic and copies ran while one was open for 11% of the time, Pallas kernels for 0%

profile of v1, /device:TPU:1, one launch (start us, length us, event | category | flops | bytes accessed | tf_op | source)
XLA Modules:
  0.0 302.0 jit_solution(7720405257235284247)
XLA Ops:
  6.5 0.0 copy-start
  6.5 0.0 all-gather.4.cloned.1.call-start
  6.6 0.7 all-gather.4.cloned.1.call-update
  7.3 0.0 all-gather.6.cloned.1.call-start
  7.3 0.7 all-gather.6.cloned.1.call-update
  8.0 0.0 copy-done.4
  8.1 0.1 slice.144
  8.1 4.5 %collective-permute-start.1 = (bf16[15]{0:T(256)(128)(2,1)S(1)}, bf16[15]{0:T(256)(128)(2,1)S(1)}, u32[]{:S(2)}, u32[]{:S(2)}) collective-permute-start(bf16[15]{0:T(256)(128)(2,1)S(1)} %slice.144), channel_id=1, source_target_pairs={{0,4},{4,8},{8,12},{12,16},{16,20},{20,24},{24,28},{28,32},{32,36}... | collective-permute-start | bytes 98 | tf_op jit(solution)/shard_map/ppermute | solution.py:15
  12.6 0.0 copy-done.2
  12.6 1.9 collective-permute-start
  14.6 0.0 collective-permute-done.1
  14.6 0.1 pad_maximum_fusion
  14.7 0.1 convert_add_fusion.1
  14.8 0.9 collective-permute-done
  15.7 0.1 maximum_convert_fusion
  15.8 0.0 copy-done
  15.8 4.4 %convolution_convert_fusion = bf16[512,2048]{1,0:T(8,128)(2,1)} fusion(bf16[512,2048]{1,0:T(8,128)(2,1)S(1)} %copy-done, f32[512]{0:T(512)S(1)} %copy-done.8, bf16[512,256]{1,0:T(8,128)(2,1)S(1)} %copy-done.2, f32[527,256]{1,0:T(8,128)S(1)} %maximum_convert_fusion, bf16[1,256,512]{2,1,0:T(8,128)(2,1)S(1)} %copy-done.7, f32[512]{0:T(512)S(1)} %get-tuple-element.9, ...), kind=kOutput, calls=%fused_computation.4 | convolution fusion | flops 1214119936 | bytes 13119488 | tf_op jit(solution)/shard_map/dot_general | solution.py:93
  20.2 4.5 %all-to-all-start = ((bf16[4,128,2048]{2,1,0:T(8,128)(2,1)}), bf16[4,128,2048]{2,1,0:T(8,128)(2,1)}, u32[]{:S(2)}, u32[]{:S(2)}) async-start(bf16[4,128,2048]{2,1,0:T(8,128)(2,1)} %bitcast.84), calls=%async_computation | async-start | bytes 4194304 | tf_op jit(solution)/shard_map/all_to_all | solution.py:25
  24.7 0.0 all-gather.8.cloned.1.call-start
  24.8 0.7 all-gather.8.cloned.1.call-update
  25.5 0.7 broadcast_multiply_fusion
  26.2 0.1 copy.27
  26.3 0.1 reshape.206
  26.4 0.1 eq.103
  26.6 0.6 reduce-window.6
  27.2 0.2 slice_reduce_fusion
  27.4 0.1 fusion.99
  27.5 0.2 fusion.52
  27.7 0.2 broadcast_in_dim.172
  27.8 0.2 select_reduce_fusion
  28.0 0.1 reduce_sum.53
  28.2 0.1 reshape.214
  28.3 0.0 copy-start.3
  28.3 43.3 %all-to-all-done = bf16[4,128,2048]{2,1,0:T(8,128)(2,1)} async-done(((bf16[4,128,2048]{2,1,0:T(8,128)(2,1)}), bf16[4,128,2048]{2,1,0:T(8,128)(2,1)}, u32[]{:S(2)}, u32[]{:S(2)}) %all-to-all-start) | async-done | bytes 2097184 | tf_op jit(solution)/shard_map/all_to_all | solution.py:25
  71.6 2.1 convert_reduce_fusion
  73.7 1.3 fusion.5
  75.0 0.2 fusion.7
  75.2 3.1 %gather_fusion = bf16[384,2048]{1,0:T(8,128)(2,1)} fusion(bf16[128,2048]{1,0:T(8,128)(2,1)S(1)} %fusion.7, s32[1024]{0:T(1024)S(1)} %pad_clamp_fusion.1), kind=kCustom, calls=%fused_computation | custom fusion | bytes 3147264 | tf_op jit(solution)/shard_map/gather | solution.py:106
  78.3 3.7 %reshape.213 = bf16[64,1,6,2048]{3,2,0,1:T(8,128)(2,1)} reshape(bf16[384,2048]{1,0:T(8,128)(2,1)} %gather_fusion) | data formatting | bytes 3145728 | tf_op jit(solution)/shard_map/gather | solution.py:106
  82.0 1.8 select_bitcast_fusion
  83.9 64.7 %all_to_all.15 = bf16[64,1,6,2048]{3,2,1,0:T(8,128)(2,1)} all-to-all(bf16[64,1,6,2048]{3,2,1,0:T(8,128)(2,1)S(1)} %select_bitcast_fusion), channel_id=1, replica_groups=mesh['sp'=64,'tp'=4] {'sp'}, dimensions={0} | all-to-all | bytes 3145728 | tf_op jit(solution)/shard_map/all_to_all | solution.py:107
  148.6 3.7 %reshape.208 = bf16[384,2048]{1,0:T(8,128)(2,1)} reshape(bf16[64,1,6,2048]{3,2,1,0:T(8,128)(2,1)} %all_to_all.15) | data formatting | bytes 3145728 | tf_op jit(solution)/shard_map/reshape | solution.py:108
  152.3 3.4 %fusion.9 = f32[384,256]{1,0:T(8,128)} fusion(bf16[384,2048]{1,0:T(8,128)(2,1)} %reshape.208, bf16[4,2048,256]{2,1,0:T(8,128)(2,1)} %all-gather.4.cloned.1.call-done), kind=kOutput, calls=%fused_computation.31 | convolution fusion | flops 402653184 | bytes 3014656 | tf_op jit(solution)/shard_map/dot_general | solution.py:111
  155.7 0.0 copy-done.1
  155.7 2.7 fusion.10
  158.5 1.4 fusion.11
  159.8 0.6 fusion.12
  160.4 0.0 all-gather.6.cloned.1.call-done
  160.4 31.0 %all-gather.8.cloned.1.call-done = bf16[4,256,2048]{2,1,0:T(8,128)(2,1)} async-done(((bf16[1,256,2048]{2,1,0:T(8,128)(2,1)}), bf16[4,256,2048]{2,1,0:T(8,128)(2,1)}) %all-gather.8.cloned.1.call-update) | async-done | bytes 4194320 | tf_op jit(solution)/shard_map/all_gather | solution.py:67
  191.5 5.2 %convolution_convert_fusion.3 = bf16[384,2048]{1,0:T(8,128)(2,1)} fusion(bf16[384,2048]{1,0:T(8,128)(2,1)} %reshape.208, bf16[4,256,2048]{2,1,0:T(8,128)(2,1)} %all-gather.8.cloned.1.call-done, bf16[4,2048,256]{2,1,0:T(8,128)(2,1)} %all-gather.6.cloned.1.call-done, f32[384,256]{1,0:T(8,128)} %fusion.11), kind=kOutput, calls=%fused_computation.7 | convolution fusion | flops 806682624 | bytes 5636096 | tf_op jit(solution)/shard_map/dot_general | solution.py:114
  196.6 5.1 %convolution_convert_fusion.2 = bf16[384,2048]{1,0:T(8,128)(2,1)} fusion(bf16[384,2048]{1,0:T(8,128)(2,1)} %reshape.208, bf16[4,256,2048]{2,1,0:T(8,128)(2,1)} %all-gather.8.cloned.1.call-done, bf16[4,2048,256]{2,1,0:T(8,128)(2,1)} %all-gather.6.cloned.1.call-done, f32[384,256]{1,0:T(8,128)} %fusion.10), kind=kOutput, calls=%fused_computation.6 | convolution fusion | flops 806682624 | bytes 5636096 | tf_op jit(solution)/shard_map/dot_general | solution.py:114
  201.7 5.1 %convolution_convert_fusion.1 = bf16[384,2048]{1,0:T(8,128)(2,1)} fusion(bf16[384,2048]{1,0:T(8,128)(2,1)} %reshape.208, bf16[4,256,2048]{2,1,0:T(8,128)(2,1)} %all-gather.8.cloned.1.call-done, bf16[4,2048,256]{2,1,0:T(8,128)(2,1)} %all-gather.6.cloned.1.call-done, f32[384,256]{1,0:T(8,128)} %fusion.9), kind=kOutput, calls=%fused_computation.5 | convolution fusion | flops 806682624 | bytes 5636096 | tf_op jit(solution)/shard_map/dot_general | solution.py:114
  206.8 6.4 %add_convert_fusion = bf16[384,2048]{1,0:T(8,128)(2,1)} fusion(bf16[384,2048]{1,0:T(8,128)(2,1)} %convolution_convert_fusion.1, bf16[384,2048]{1,0:T(8,128)(2,1)} %convolution_convert_fusion.2, bf16[384,2048]{1,0:T(8,128)(2,1)} %convolution_convert_fusion.3, bf16[4,256,2048]{2,1,0:T(8,128)(2,1)} %all-gather.8.cloned.1.call-done, ...), kind=kOutput, calls=%fused_computation.3 | convolution fusion | flops 812974080 | bytes 10354688 | tf_op jit(solution)/shard_map/dot_general | solution.py:114
  213.3 3.7 %reshape.209 = bf16[64,1,6,2048]{3,2,0,1:T(8,128)(2,1)} reshape(bf16[384,2048]{1,0:T(8,128)(2,1)} %add_convert_fusion) | data formatting | bytes 3145728 | tf_op jit(solution)/shard_map/reshape | solution.py:116
  217.0 11.2 %all-to-all-start.2 = ((bf16[64,1,6,2048]{3,2,1,0:T(8,128)(2,1)}), bf16[64,1,6,2048]{3,2,1,0:T(8,128)(2,1)}, u32[]{:S(2)}, u32[]{:S(2)}) async-start(bf16[64,1,6,2048]{3,2,1,0:T(8,128)(2,1)} %bitcast.83), calls=%async_computation.2 | async-start | bytes 4194304 | tf_op jit(solution)/shard_map/all_to_all | solution.py:117
  228.1 0.1 copy.32
  228.2 0.1 mul.116
  228.4 0.1 copy.26
  228.5 49.2 %all-to-all-done.2 = bf16[64,1,6,2048]{3,2,1,0:T(8,128)(2,1)} async-done(((bf16[64,1,6,2048]{3,2,1,0:T(8,128)(2,1)}), bf16[64,1,6,2048]{3,2,1,0:T(8,128)(2,1)}, u32[]{:S(2)}, u32[]{:S(2)}) %all-to-all-start.2) | async-done | bytes 1572896 | tf_op jit(solution)/shard_map/all_to_all | solution.py:117
  277.7 3.7 %reshape.210 = bf16[384,2048]{1,0:T(8,128)(2,1)} reshape(bf16[64,1,6,2048]{3,2,1,0:T(8,128)(2,1)} %all-to-all-done.2) | data formatting | bytes 3145728 | tf_op jit(solution)/shard_map/reshape | solution.py:118
  281.4 4.9 %gather_fusion.1 = bf16[256,2048]{1,0:T(8,128)(2,1)} fusion(bf16[384,2048]{1,0:T(8,128)(2,1)} %reshape.210, s32[1024]{0:T(1024)S(1)} %pad_clamp_fusion), kind=kCustom, calls=%fused_computation.1 | custom fusion | bytes 2098176 | tf_op jit(solution)/shard_map/gather | solution.py:119
  286.4 3.4 %reshape.211 = f32[128,2,2048]{2,1,0:T(2,128)} reshape(bf16[256,2048]{1,0:T(8,128)(2,1)} %gather_fusion.1) | data formatting | bytes 3145728 | tf_op jit(solution)/shard_map/convert_element_type | solution.py:119
  289.8 4.8 %multiply_reduce_fusion = f32[128,2048]{1,0:T(8,128)S(1)} fusion(f32[128,2,2048]{2,1,0:T(2,128)} %reshape.211, f32[128,2]{1,0:T(8,128)S(1)} %copy.26), kind=kLoop, calls=%fused_computation.9 | loop fusion | flops 786432 | bytes 3146752 | tf_op jit(solution)/shard_map/reduce_sum | solution.py:120
  294.6 0.9 fusion.8
  (25 shorter events, 0.2 us)
Async XLA Ops:
  6.5 9.2 %copy-start = (bf16[512,2048]{1,0:T(8,128)(2,1)S(1)}, bf16[512,2048]{1,0:T(8,128)(2,1)}, u32[]{:S(2)}) copy-start(bf16[512,2048]{1,0:T(8,128)(2,1)} %param.17) | copy-start | bytes 6291460
  6.5 1.5 copy-start.4
  6.5 6.1 %copy-start.2 = (bf16[512,256]{1,0:T(8,128)(2,1)S(1)}, bf16[512,256]{1,0:T(8,128)(2,1)}, u32[]{:S(2)}) copy-start(bf16[512,256]{1,0:T(8,128)(2,1)} %param.13) | copy-start | bytes 786436
  6.5 9.2 %copy-start.8 = (f32[512]{0:T(512)S(1)}, f32[512]{0:T(512)}, u32[]{:S(2)}) copy-start(f32[512]{0:T(512)} %param.16) | copy-start | bytes 6148
  6.5 9.3 %copy-start.7 = (bf16[1,256,512]{2,1,0:T(8,128)(2,1)S(1)}, bf16[1,256,512]{2,1,0:T(8,128)(2,1)}, u32[]{:S(2)}) copy-start(bf16[1,256,512]{2,1,0:T(8,128)(2,1)} %param.15) | copy-start | bytes 786436
  6.5 145.7 %all-gather.4.cloned.1.call-start = ((), (), s32[]{:S(2)}) async-start(), calls=%async_computation.3 | async-start | bytes 5242880 | tf_op jit(solution)/shard_map/all_gather | solution.py:65
  7.3 153.2 %all-gather.6.cloned.1.call-start = ((), (), s32[]{:S(2)}) async-start(), calls=%async_computation.4 | async-start | bytes 5242880 | tf_op jit(solution)/shard_map/all_gather | solution.py:66
  8.1 6.5 %collective-permute-start.1 = (bf16[15]{0:T(256)(128)(2,1)S(1)}, bf16[15]{0:T(256)(128)(2,1)S(1)}, u32[]{:S(2)}, u32[]{:S(2)}) collective-permute-start(bf16[15]{0:T(256)(128)(2,1)S(1)} %slice.144), channel_id=1, source_target_pairs={{0,4},{4,8},{8,12},{12,16},{16,20},{20,24},{24,28},{28,32},{32,36}... | collective-permute-start | bytes 98 | tf_op jit(solution)/shard_map/ppermute | solution.py:15
  12.6 3.1 %collective-permute-start = (bf16[15,256]{1,0:T(8,128)(2,1)S(1)}, bf16[15,256]{1,0:T(8,128)(2,1)S(1)}, u32[]{:S(2)}, u32[]{:S(2)}) collective-permute-start(bf16[15,256]{1,0:T(8,128)(2,1)S(1)} %slice.142), channel_id=1, source_target_pairs={{0,4},{4,8},{8,12},{12,16},{16,20},{20,24},{24,28},{28,32},{32,36}... | collective-permute-start | bytes 23048 | tf_op jit(solution)/shard_map/ppermute | solution.py:15
  20.2 51.4 %all-to-all-start = ((bf16[4,128,2048]{2,1,0:T(8,128)(2,1)}), bf16[4,128,2048]{2,1,0:T(8,128)(2,1)}, u32[]{:S(2)}, u32[]{:S(2)}) async-start(bf16[4,128,2048]{2,1,0:T(8,128)(2,1)} %bitcast.84), calls=%async_computation | async-start | bytes 4194304 | tf_op jit(solution)/shard_map/all_to_all | solution.py:25
  24.7 166.8 %all-gather.8.cloned.1.call-start = ((), (), s32[]{:S(2)}) async-start(), calls=%async_computation.5 | async-start | bytes 5242880 | tf_op jit(solution)/shard_map/all_gather | solution.py:67
  28.3 46.7 %copy-start.3 = (f32[2048]{0:T(1024)S(1)}, f32[2048]{0:T(1024)}, u32[]{:S(2)}) copy-start(f32[2048]{0:T(1024)} %param.18) | copy-start | bytes 24580
  152.3 3.4 %copy-start.1 = (bf16[384,2048]{1,0:T(8,128)(2,1)S(1)}, bf16[384,2048]{1,0:T(8,128)(2,1)}, u32[]{:S(2)}) copy-start(bf16[384,2048]{1,0:T(8,128)(2,1)} %reshape.208) | copy-start | bytes 4718596
  155.7 2.8 copy-start.6
  217.0 11.4 %copy-start.5 = (f32[128,2]{0,1:T(2,128)S(1)}, f32[128,2]{0,1:T(2,128)}, u32[]{:S(2)}) copy-start(f32[128,2]{0,1:T(2,128)} %param.20) | copy-start | bytes 3076
  217.0 60.8 %all-to-all-start.2 = ((bf16[64,1,6,2048]{3,2,1,0:T(8,128)(2,1)}), bf16[64,1,6,2048]{3,2,1,0:T(8,128)(2,1)}, u32[]{:S(2)}, u32[]{:S(2)}) async-start(bf16[64,1,6,2048]{3,2,1,0:T(8,128)(2,1)} %bitcast.83), calls=%async_computation.2 | async-start | bytes 4194304 | tf_op jit(solution)/shard_map/all_to_all | solution.py:117
Sparse Core Ops, SparseCore 0:
  9.2 75.9 all-gather.3
  87.0 51.4 all-gather.5
  140.3 51.1 all-gather.7

commit v2 on v0

v2 whole, which is shorter than its diff:
```python
import functools

import jax
import jax.numpy as jnp
from jax import lax
from jax.experimental import pallas as pl
from jax.experimental.pallas import tpu as pltpu
from jax.sharding import PartitionSpec as P

MESH = pl.DeviceIdType.MESH
SPAN = 16
EPS = 1e-06
LANES = 128
HALVES = 2


def passed_along(value, axis, by):
    length = lax.axis_size(axis)
    pairs = [(i, i + by) for i in range(length) if 0 <= i + by < length]
    return lax.ppermute(value, axis, pairs)


def slot_table(route_block, expert_count, capacity, top_count):
    flattened = route_block.reshape(-1)
    one_hot = (flattened[:, None] == jnp.arange(expert_count, dtype=jnp.int32)[None, :]).astype(
        jnp.int32
    )
    ranking = jnp.sum((jnp.cumsum(one_hot, axis=0) - one_hot) * one_hot, axis=1)
    target_slot = flattened * capacity + ranking
    matches = target_slot[None, :] == jnp.arange(expert_count * capacity, dtype=jnp.int32)[:, None]
    sources = jnp.sum(
        jnp.where(matches, jnp.arange(flattened.shape[0], dtype=jnp.int32)[None, :], 0), axis=1
    )
    return (target_slot, sources // top_count)


def layer_kernel(
    experts,
    capacity,
    tp_count,
    source_ref,
    slot_ref,
    weight_ref,
    part_hbm,
    stream_hbm,
    gain_ref,
    gate_hbm,
    up_hbm,
    down_hbm,
    out_ref,
    tiles,
    stream_v,
    mixed,
    tokens,
    rounded,
    packed,
    arrived,
    wide,
    inputs,
    all_gate,
    all_up,
    all_down,
    hidden,
    shaped,
    sending,
    returned,
    picked_from,
    combined,
    local_sem,
    tile_send,
    tile_recv,
    row_send,
    row_recv,
    out_send,
    out_recv,
    own_send,
    own_recv,
    fwd_send,
    fwd_recv,
):
    sp, tp = lax.axis_index("sp"), lax.axis_index("tp")
    above, below, across = (tp + 1) % tp_count, (tp + tp_count - 1) % tp_count, (tp + 2) % tp_count
    rows, width = stream_v.shape
    blocks = width // LANES
    slots = experts * capacity
    depth = width // HALVES
    ff_part = hidden.shape[2]
    ff_half = ff_part // HALVES
    columns = width // HALVES
    col_blocks = columns // LANES

    def remote(src, dst, send, recv, target):
        return pltpu.make_async_remote_copy(
            src_ref=src,
            dst_ref=dst,
            send_sem=send,
            recv_sem=recv,
            device_id=target,
            device_id_type=MESH,
        )

    barrier = pltpu.get_barrier_semaphore()
    for step in range(1, tp_count):
        pl.semaphore_signal(
            barrier, inc=1, device_id=(sp, (tp + step) % tp_count), device_id_type=MESH
        )

    @pl.loop(1, experts)
    def _(step):
        pl.semaphore_signal(
            barrier, inc=1, device_id=((sp + step) % experts, tp), device_id_type=MESH
        )

    loads = [
        pltpu.make_async_copy(part_hbm.at[tp], tiles.at[tp], local_sem.at[0]),
        pltpu.make_async_copy(stream_hbm, stream_v, local_sem.at[1]),
        pltpu.make_async_copy(gate_hbm, all_gate.at[tp], local_sem.at[2]),
        pltpu.make_async_copy(up_hbm, all_up.at[tp], local_sem.at[3]),
        pltpu.make_async_copy(down_hbm, all_down.at[tp], local_sem.at[4]),
    ]
    for load in loads:
        load.start()
    pl.semaphore_wait(barrier, experts - 1 + tp_count - 1)

    for step in (1, 3, 2):
        owner = (tp + step) % tp_count
        remote(part_hbm.at[owner], tiles.at[tp], tile_send, tile_recv, (sp, owner)).start()

    def region(which, block, half):
        if which == 0:
            return all_gate.at[block, pl.ds(half * depth, depth)]
        if which == 1:
            return all_up.at[block, pl.ds(half * depth, depth)]
        return all_down.at[block, :, pl.ds(half * columns, columns)]

    def own_source(which, half):
        if which == 0:
            return gate_hbm.at[pl.ds(half * depth, depth)]
        if which == 1:
            return up_hbm.at[pl.ds(half * depth, depth)]
        return down_hbm.at[:, pl.ds(half * columns, columns)]

    def own_copy(which, half, way):
        target = above if way == 0 else below
        return remote(
            own_source(which, half),
            region(which, tp, half),
            own_send.at[way, which, half],
            own_recv.at[way, which, half],
            (sp, target),
        )

    def send_own(which, half):
        for way in range(2):
            own_copy(which, half, way).start()

    def wait_own(which, half, way):
        own_copy(which, half, way).wait_recv()

    def fwd_copy(which, part, way):
        block = below if way == 0 else above
        half = 1 - way
        if which == 2:
            ref = all_down.at[block, pl.ds(half * ff_half, ff_half), pl.ds(part * columns, columns)]
        else:
            ref = region(which, block, half)
        target = above if way == 0 else below
        return remote(
            ref, ref, fwd_send.at[way, which, part], fwd_recv.at[way, which, part], (sp, target)
        )

    for which in range(2):
        for half in range(HALVES):
            send_own(which, half)

    loads[0].wait()
    loads[1].wait()
    summed_tiles = remote(
        tiles.at[pl.ds(0, tp_count - 1)],
        tiles.at[pl.ds(0, tp_count - 1)],
        tile_send,
        tile_recv,
        (sp, above),
    )
    summed_tiles.wait_recv()

    step_rows = 16

    @pl.loop(0, rows // step_rows)
    def _(i):
        at = pl.ds(pl.multiple_of(i * step_rows, step_rows), step_rows)
        total = tiles[0, at, :].astype(jnp.float32)
        for k in range(1, tp_count):
            total = total + tiles[k, at, :].astype(jnp.float32)
        here = (stream_v[at, :].astype(jnp.float32) + total).astype(jnp.bfloat16)
        here = here.astype(jnp.float32)
        mixed[at, :] = here
        scale = lax.rsqrt(jnp.mean(here * here, axis=1, keepdims=True) + EPS)
        normed = here * scale * gain_ref[...]
        for c in range(blocks):
            tokens[pl.ds(i * (step_rows * blocks) + c, step_rows, stride=blocks), :] = normed[
                :, c * LANES : (c + 1) * LANES
            ]

    @pl.loop(0, rows, unroll=4)
    def _(t):
        rounded[t] = tokens[pl.ds(pl.multiple_of(t * blocks, blocks), blocks), :].astype(
            jnp.bfloat16
        )

    @pl.loop(0, slots, unroll=4)
    def _(s):
        packed[s] = rounded[source_ref[s]]

    @pl.loop(1, experts)
    def _(step):
        peer = (sp + step) % experts
        remote(
            packed.at[pl.ds(peer * capacity, capacity)],
            arrived.at[pl.ds(sp * capacity, capacity)],
            row_send,
            row_recv,
            (peer, tp),
        ).start()

    @pl.loop(0, capacity)
    def _(r):
        arrived[sp * capacity + r] = packed[sp * capacity + r]

    for which in range(2):
        wait_own(which, 1, 0)
        fwd_copy(which, 0, 0).start()
        wait_own(which, 0, 1)
        fwd_copy(which, 0, 1).start()
        wait_own(which, 0, 0)
        wait_own(which, 1, 1)
    for half in range(HALVES):
        send_own(2, half)

    all_rows = remote(
        packed.at[pl.ds(0, (experts - 1) * capacity)],
        arrived.at[pl.ds(0, (experts - 1) * capacity)],
        row_send,
        row_recv,
        (sp, above),
    )
    all_rows.wait_recv()

    @pl.loop(0, slots, unroll=4)
    def _(s):
        wide[pl.ds(pl.multiple_of(s * blocks, blocks), blocks), :] = arrived[s].astype(jnp.float32)

    for c in range(blocks):
        inputs[:, c * LANES : (c + 1) * LANES] = wide[pl.ds(c, slots, stride=blocks), :].astype(
            jnp.bfloat16
        )

    loads[2].wait()
    loads[3].wait()
    loads[4].wait()

    def run_hidden(block):
        gate_pre = jnp.dot(inputs[...], all_gate[block], preferred_element_type=jnp.float32)
        up_pre = jnp.dot(inputs[...], all_up[block], preferred_element_type=jnp.float32)
        hidden[block] = (jax.nn.silu(gate_pre) * up_pre).astype(jnp.bfloat16)

    run_hidden(tp)
    run_hidden(below)
    run_hidden(above)
    for which in range(2):
        for way in range(2):
            fwd_copy(which, 0, way).wait_recv()
    run_hidden(across)

    row_step = 128
    for half in range(HALVES):
        for way in range(2):
            wait_own(2, half, way)
            fwd_copy(2, half, way).start()
        for way in range(2):
            fwd_copy(2, half, way).wait_recv()

        @pl.loop(0, slots // row_step)
        def _(i):
            at = pl.ds(pl.multiple_of(i * row_step, row_step), row_step)
            total = jnp.zeros((row_step, columns), jnp.float32)
            for block in range(tp_count):
                piece = jnp.dot(
                    hidden[block, at, :],
                    all_down[block, :, half * columns : (half + 1) * columns],
                    preferred_element_type=jnp.float32,
                )
                total = total + piece.astype(jnp.bfloat16).astype(jnp.float32)
            for c in range(col_blocks):
                shaped[pl.ds(i * (row_step * col_blocks) + c, row_step, stride=col_blocks), :] = (
                    total[:, c * LANES : (c + 1) * LANES]
                )

        lines = capacity * col_blocks

        @pl.loop(0, experts)
        def _(j):
            sending[half, j] = shaped[pl.ds(pl.multiple_of(j * lines, lines), lines), :].astype(
                jnp.bfloat16
            )

        @pl.loop(1, experts)
        def _(step):
            peer = (sp + step) % experts
            remote(
                sending.at[half, peer],
                returned.at[half, sp],
                out_send.at[half],
                out_recv.at[half],
                (peer, tp),
            ).start()

        returned[half, sp] = sending[half, sp]

    def all_out(half):
        return remote(
            sending.at[half, pl.ds(0, experts - 1)],
            returned.at[half, pl.ds(0, experts - 1)],
            out_send.at[half],
            out_recv.at[half],
            (sp, above),
        )

    for half in range(HALVES):
        all_out(half).wait_recv()

        @pl.loop(0, experts)
        def _(j):
            picked_from[pl.ds(j * capacity, capacity)] = (
                returned[half, j].astype(jnp.float32).reshape(capacity, col_blocks, LANES)
            )

        @pl.loop(0, rows, unroll=4)
        def _(t):
            combined[pl.ds(pl.multiple_of(t * col_blocks, col_blocks), col_blocks), :] = (
                weight_ref[2 * t] * picked_from[slot_ref[2 * t]]
                + weight_ref[2 * t + 1] * picked_from[slot_ref[2 * t + 1]]
            )

        for c in range(col_blocks):
            at = slice(half * columns + c * LANES, half * columns + (c + 1) * LANES)
            out_ref[:, at] = (
                mixed[:, at] + combined[pl.ds(c, rows, stride=col_blocks), :]
            ).astype(jnp.bfloat16)

    summed_tiles.wait_send()
    all_rows.wait_send()
    for half in range(HALVES):
        all_out(half).wait_send()
        for way in range(2):
            for which in range(3):
                own_copy(which, half, way).wait_send()
    for way in range(2):
        for half in range(HALVES):
            fwd_copy(2, half, way).wait_send()
        fwd_copy(0, 0, way).wait_send()
        fwd_copy(1, 0, way).wait_send()


def per_device(
    stream,
    pool_in,
    doc_ids,
    pool_map,
    pool_scale,
    out_weight,
    norm_gain,
    routes,
    route_weight,
    expert_gate,
    expert_up,
    expert_down,
):
    row_count = pool_in.shape[0]
    model_width = stream.shape[1]
    top_count = routes.shape[1]
    tp_count = lax.axis_size("tp")
    expert_count = lax.axis_size("sp")
    quarter = row_count // tp_count
    capacity = max(2, 3 * top_count * quarter // (2 * expert_count))
    ff_part = expert_gate.shape[2]
    reach_rows = SPAN - 1
    tail_rows = (
        pool_in[row_count - reach_rows :],
        doc_ids[row_count - reach_rows :].astype(jnp.bfloat16),
    )
    prior_rows, prior_docs = passed_along((tail_rows[0], tail_rows[1]), "sp", 1)
    extended = jnp.concatenate([prior_rows, pool_in], axis=0).astype(jnp.float32)
    extended_docs = jnp.concatenate([prior_docs.astype(jnp.float32), doc_ids.astype(jnp.float32)])
    own_docs = doc_ids.astype(jnp.float32)
    window = jnp.left_shift(jnp.int32(2), lax.axis_index("tp"))
    positions = lax.axis_index("sp") * row_count + jnp.arange(row_count, dtype=jnp.int32)
    running = jnp.zeros(pool_in.shape, jnp.float32)
    counts = jnp.zeros((row_count,), jnp.float32)
    for offset in range(reach_rows + 1):
        begin_row = reach_rows - offset
        piece_rows = extended[begin_row : begin_row + row_count]
        piece_docs = extended_docs[begin_row : begin_row + row_count]
        in_window = (offset < window) & (positions - offset >= 0) & (piece_docs == own_docs)
        running = running + jnp.where(in_window[:, None], piece_rows, 0.0)
        counts = counts + in_window.astype(jnp.float32)
    pooled = (running / counts[:, None] - pool_in.astype(jnp.float32)).astype(jnp.bfloat16)
    branch = (jnp.dot(pooled, pool_map[0], preferred_element_type=jnp.float32) * pool_scale).astype(
        jnp.bfloat16
    )
    partial = jnp.dot(branch, out_weight, preferred_element_type=jnp.float32).astype(jnp.bfloat16)
    partial = partial.reshape(tp_count, quarter, model_width)

    own_routes = lax.dynamic_slice_in_dim(routes, lax.axis_index("tp") * quarter, quarter, 0)
    own_slots, own_sources = slot_table(own_routes, expert_count, capacity, top_count)

    slots = expert_count * capacity
    blocks = model_width // LANES
    half_blocks = blocks // HALVES
    bf16, f32 = jnp.bfloat16, jnp.float32
    vmem, dma = pltpu.VMEM, pltpu.SemaphoreType.DMA
    smem_spec = pl.BlockSpec(memory_space=pltpu.SMEM)
    any_spec = pl.BlockSpec(memory_space=pl.ANY)
    vmem_spec = pl.BlockSpec(memory_space=pltpu.VMEM)
    return pl.pallas_call(
        functools.partial(layer_kernel, expert_count, capacity, tp_count),
        out_shape=jax.ShapeDtypeStruct((quarter, model_width), bf16),
        in_specs=[smem_spec] * 3 + [any_spec] * 2 + [vmem_spec] + [any_spec] * 3,
        out_specs=vmem_spec,
        scratch_shapes=[
            vmem((tp_count, quarter, model_width), bf16),
            vmem((quarter, model_width), bf16),
            vmem((quarter, model_width), f32),
            vmem((quarter * blocks, LANES), f32),
            vmem((quarter, blocks, LANES), bf16),
            vmem((slots, blocks, LANES), bf16),
            vmem((slots, blocks, LANES), bf16),
            vmem((slots * blocks, LANES), f32),
            vmem((slots, model_width), bf16),
            vmem((tp_count, model_width, ff_part), bf16),
            vmem((tp_count, model_width, ff_part), bf16),
            vmem((tp_count, ff_part, model_width), bf16),
            vmem((tp_count, slots, ff_part), bf16),
            vmem((slots * half_blocks, LANES), f32),
            vmem((HALVES, expert_count, capacity * half_blocks, LANES), bf16),
            vmem((HALVES, expert_count, capacity * half_blocks, LANES), bf16),
            vmem((slots, half_blocks, LANES), f32),
            vmem((quarter * half_blocks, LANES), f32),
            dma((5,)),
            dma,
            dma,
            dma,
            dma,
            dma((HALVES,)),
            dma((HALVES,)),
            dma((2, 3, HALVES)),
            dma((2, 3, HALVES)),
            dma((2, 3, HALVES)),
            dma((2, 3, HALVES)),
        ],
        compiler_params=pltpu.CompilerParams(
            collective_id=0, has_side_effects=True, vmem_limit_bytes=56 * 1024 * 1024
        ),
    )(
        own_sources,
        own_slots,
        route_weight.reshape(-1),
        partial,
        stream,
        norm_gain.reshape(1, -1),
        expert_gate[0],
        expert_up[0],
        expert_down[0],
    )


def solution(mesh):
    in_specs = (
        P(("sp", "tp"), None),
        P("sp", "tp"),
        P("sp"),
        P("tp", None, None),
        P("tp"),
        P("tp", None),
        P(),
        P("sp", None),
        P(("sp", "tp"), None),
        P("sp", None, "tp"),
        P("sp", None, "tp"),
        P("sp", "tp", None),
    )
    out_specs = P(("sp", "tp"), None)
    return jax.shard_map(
        per_device, mesh=mesh, in_specs=in_specs, out_specs=out_specs, check_vma=False
    )
```

time: 379 us -> 195 us (0.51)
  Pallas kernels: 0 us -> 173 us
  blocking collectives: 136 us -> 0 us
  waiting for transfers between devices: 136 us -> 0.01 us
  local copies, waits for them, and re-layouts: 40.9 us -> 5.44 us
  starting transfers between devices: 22.9 us -> 6.39 us
  between operations: 13.7 us -> 0.13 us
  other arithmetic: 14.2 us -> 4.24 us
  matrix products: 14.3 us -> 5.39 us
    pallas_call x0 -> x1, Pallas kernels: none -> 173 us  [per_device(): pl.pallas_call(functools.partial(layer_kernel, expert_count, capacity, tp...]
    all_to_all x2 -> x0, blocking collectives: 136 us -> none  [the longest x1 73.4 us: sum_at_owner(): lax.all_to_all(cut_along(value, dim, length), axis, 0, 0, tiled=True)]
    all_to_all x2 -> x0, waiting for transfers between devices: 72.1 us -> none  [the longest x1 49.2 us: per_device(): lax.all_to_all(summed, 'sp', split_axis=0, concat_axis=0, tiled=True)]
    all_gather x1 -> x0, waiting for transfers between devices: 64 us -> none  [per_device(): arrived = lax.all_gather(arrived, 'tp', axis=1, tiled=True)]
    all_to_all x2 -> x0, starting transfers between devices: 16.5 us -> none  [the longest x1 12.3 us: per_device(): lax.all_to_all(summed, 'sp', split_axis=0, concat_axis=0, tiled=True)]
    reshape x2 -> x1, local copies, waits for them, and re-layouts: 13.7 us -> 0.72 us  [per_device(): route_weight.reshape(-1)]
    all_gather x1 -> x0, local copies, waits for them, and re-layouts: 9.61 us -> none  [per_device(): arrived = lax.all_gather(arrived, 'tp', axis=1, tiled=True)]
    dot_general x3 -> x0, matrix products: 8.89 us -> none  [the longest x1 4.8 us: per_device(): jnp.dot(stacked, expert_gate[0], preferred_element_type=jnp.float32)]
  transfers between devices with their start and end apart: 5 -> 2, of which waited for: 4 -> 0; matrix products, arithmetic and copies ran while one was open for 1% -> 3% of each run, Pallas kernels for 0% -> 0%
where the time goes in v2:
time: 195 us; the launch traced here: 194 us
  Pallas kernels  173 us (89%)
  starting transfers between devices  6.39 us (3%)
  local copies, waits for them, and re-layouts  5.44 us (3%)
  matrix products  5.39 us (3%)
  other arithmetic  4.24 us (2%)
    pallas_call x1, Pallas kernels, per_device(): pl.pallas_call(functools.partial(layer_kernel, expert_count, capacity, tp...  173 us
    ppermute x2, starting transfers between devices, passed_along(): return lax.ppermute(value, axis, pairs)  6.39 us
    dot_general x1, matrix products, per_device(): jnp.dot(branch, out_weight, preferred_element_type=jnp.float32)  5.39 us
  transfers between devices with their start and end apart: 2, of which 0 were waited for; matrix products, arithmetic and copies ran while one was open for 3% of the time, Pallas kernels for 0%

profile of v2, /device:TPU:1, one launch (start us, length us, event | category | flops | bytes accessed | tf_op | source)
XLA Modules:
  0.0 194.4 jit_solution(2752328981302187641)
XLA Ops:
  0.0 0.0 copy-start
  0.0 0.9 fusion.117
  0.9 0.1 slice.110
  0.9 4.5 %collective-permute-start.1 = (bf16[15]{0:T(256)(128)(2,1)S(1)}, bf16[15]{0:T(256)(128)(2,1)S(1)}, u32[]{:S(2)}, u32[]{:S(2)}) collective-permute-start(bf16[15]{0:T(256)(128)(2,1)S(1)} %slice.110), channel_id=1, source_target_pairs={{0,4},{4,8},{8,12},{12,16},{16,20},{20,24},{24,28},{28,32},{32,36}... | collective-permute-start | bytes 98 | tf_op jit(solution)/shard_map/ppermute | solution.py:20
  5.4 0.7 slice.108
  6.1 1.9 collective-permute-start
  8.1 0.7 constant_dynamic-slice_fusion
  8.7 0.1 copy.17
  8.9 0.1 eq.87
  9.0 0.1 reshape.55
  9.2 0.6 reduce-window.6
  9.8 0.2 slice_reduce_fusion
  10.0 0.1 fusion.62
  10.2 0.0 copy-start.1
  10.2 0.1 select_reduce_fusion
  10.3 0.6 add_select_fusion.source_ref
  10.9 0.8 copy.20
  11.7 0.7 reshape.57.weight_ref
  12.4 0.0 collective-permute-done.1
  12.4 0.1 pad_maximum_fusion
  12.5 0.8 convert_add_fusion
  13.3 0.0 collective-permute-done
  13.3 1.0 maximum_convert_fusion
  14.3 0.0 copy-done
  14.3 5.4 %convolution_convert_fusion = bf16[512,2048]{1,0:T(8,128)(2,1)} fusion(bf16[512,2048]{1,0:T(8,128)(2,1)S(1)} %copy-done, f32[512]{0:T(512)} %param.16, bf16[512,256]{1,0:T(8,128)(2,1)} %param.13, f32[527,256]{1,0:T(8,128)S(1)} %maximum_convert_fusion, bf16[1,256,512]{2,1,0:T(8,128)(2,1)} %param.15, f32[512]{0:T(512)S(1)} %get-tuple-element.5, ...), kind=kOutput, calls=%fused_computation | convolution fusion | flops 1214119936 | bytes 13119488 | tf_op jit(solution)/shard_map/dot_general | solution.py:411
  19.7 0.0 copy-done.1
  19.7 172.8 %shard_map.118 = bf16[128,2048]{1,0:T(8,128)(2,1)} custom-call(s32[384]{0:T(512)} %add_select_fusion.source_ref, s32[256]{0:T(256)} %copy-done.1, f32[256]{0:T(256)} %reshape.57.weight_ref, bf16[4,128,2048]{2,1,0:T(8,128)(2,1)} %bitcast.29, bf16[128,2048]{1,0:T(8,128)(2,1)} %stream_hbm.1, f32[1,2048]{1,0:T(1,128)} %bitcast.33, bf16[2048,256]{1,0:T(8,128)(2,1)} %bitcast.30, ...), custom_call_target="tpu_custom_call" | custom-call | tf_op jit(solution)/shard_map/pallas_call | solution.py:425
  192.5 1.9 copy.24
  (5 shorter events, 0.1 us)
Async XLA Ops:
  0.0 14.3 %copy-start = (bf16[512,2048]{1,0:T(8,128)(2,1)S(1)}, bf16[512,2048]{1,0:T(8,128)(2,1)}, u32[]{:S(2)}) copy-start(bf16[512,2048]{1,0:T(8,128)(2,1)} %param.17) | copy-start | bytes 6291460
  0.9 11.5 %collective-permute-start.1 = (bf16[15]{0:T(256)(128)(2,1)S(1)}, bf16[15]{0:T(256)(128)(2,1)S(1)}, u32[]{:S(2)}, u32[]{:S(2)}) collective-permute-start(bf16[15]{0:T(256)(128)(2,1)S(1)} %slice.110), channel_id=1, source_target_pairs={{0,4},{4,8},{8,12},{12,16},{16,20},{20,24},{24,28},{28,32},{32,36}... | collective-permute-start | bytes 98 | tf_op jit(solution)/shard_map/ppermute | solution.py:20
  6.1 7.2 %collective-permute-start = (bf16[15,256]{1,0:T(8,128)(2,1)S(1)}, bf16[15,256]{1,0:T(8,128)(2,1)S(1)}, u32[]{:S(2)}, u32[]{:S(2)}) collective-permute-start(bf16[15,256]{1,0:T(8,128)(2,1)S(1)} %slice.108), channel_id=1, source_target_pairs={{0,4},{4,8},{8,12},{12,16},{16,20},{20,24},{24,28},{28,32},{32,36}... | collective-permute-start | bytes 23048 | tf_op jit(solution)/shard_map/ppermute | solution.py:20
  10.2 9.6 %copy-start.1 = (s32[256]{0:T(256)}, s32[256]{0:T(256)S(1)}, u32[]{:S(2)}) copy-start(s32[256]{0:T(256)S(1)} %multiply_add_fusion.slot_ref) | copy-start | bytes 3076

commit v3 on v2

--- a/solution.py
+++ b/solution.py
@@ -8,16 +8,11 @@
 from jax.sharding import PartitionSpec as P
 
 MESH = pl.DeviceIdType.MESH
-SPAN = 16
 EPS = 1e-06
 LANES = 128
 HALVES = 2
-
-
-def passed_along(value, axis, by):
-    length = lax.axis_size(axis)
-    pairs = [(i, i + by) for i in range(length) if 0 <= i + by < length]
-    return lax.ppermute(value, axis, pairs)
+CHUNKS = 4
+LINES = 8
 
 
 def slot_table(route_block, expert_count, capacity, top_count):
@@ -41,13 +36,22 @@
     source_ref,
     slot_ref,
     weight_ref,
-    part_hbm,
+    docs_ref,
+    pool_hbm,
+    map_hbm,
+    scale_ref,
+    project_hbm,
     stream_hbm,
     gain_ref,
     gate_hbm,
     up_hbm,
     down_hbm,
     out_ref,
+    pool_rows,
+    docs,
+    pool_map,
+    project,
+    partial,
     tiles,
     stream_v,
     mixed,
@@ -67,6 +71,8 @@
     picked_from,
     combined,
     local_sem,
+    prior_send,
+    prior_recv,
     tile_send,
     tile_recv,
     row_send,
@@ -86,7 +92,7 @@
     depth = width // HALVES
     ff_part = hidden.shape[2]
     ff_half = ff_part // HALVES
-    columns = width // HALVES
+    columns = width // CHUNKS
     col_blocks = columns // LANES
 
     def remote(src, dst, send, recv, target):
@@ -112,19 +118,34 @@
         )
 
     loads = [
-        pltpu.make_async_copy(part_hbm.at[tp], tiles.at[tp], local_sem.at[0]),
+        pltpu.make_async_copy(pool_hbm, pool_rows.at[pl.ds(1, tp_count)], local_sem.at[0]),
         pltpu.make_async_copy(stream_hbm, stream_v, local_sem.at[1]),
         pltpu.make_async_copy(gate_hbm, all_gate.at[tp], local_sem.at[2]),
         pltpu.make_async_copy(up_hbm, all_up.at[tp], local_sem.at[3]),
         pltpu.make_async_copy(down_hbm, all_down.at[tp], local_sem.at[4]),
+        pltpu.make_async_copy(map_hbm, pool_map, local_sem.at[5]),
+        pltpu.make_async_copy(project_hbm, project, local_sem.at[6]),
     ]
-    for load in loads:
-        load.start()
+    for which in (0, 5, 6, 1, 2, 3, 4):
+        loads[which].start()
+    docs[1 : tp_count + 1] = docs_ref[...]
     pl.semaphore_wait(barrier, experts - 1 + tp_count - 1)
 
-    for step in (1, 3, 2):
-        owner = (tp + step) % tp_count
-        remote(part_hbm.at[owner], tiles.at[tp], tile_send, tile_recv, (sp, owner)).start()
+    following = ((sp + 1) % experts, tp)
+    prior = [
+        remote(
+            pool_hbm.at[tp_count - 1],
+            pool_rows.at[0],
+            prior_send.at[0],
+            prior_recv.at[0],
+            following,
+        ),
+        remote(
+            docs_ref.at[tp_count - 1], docs.at[0], prior_send.at[1], prior_recv.at[1], following
+        ),
+    ]
+    for copy in prior:
+        copy.start()
 
     def region(which, block, half):
         if which == 0:
@@ -153,6 +174,17 @@
     def send_own(which, half):
         for way in range(2):
             own_copy(which, half, way).start()
+
+    def send_quarter(quarter):
+        at = pl.ds(quarter * (depth // 2), depth // 2)
+        for way in range(2):
+            remote(
+                gate_hbm.at[at],
+                all_gate.at[tp, at],
+                own_send.at[way, 0, 0],
+                own_recv.at[way, 0, 0],
+                (sp, above if way == 0 else below),
+            ).start()
 
     def wait_own(which, half, way):
         own_copy(which, half, way).wait_recv()
@@ -169,11 +201,55 @@
             ref, ref, fwd_send.at[way, which, part], fwd_recv.at[way, which, part], (sp, target)
         )
 
-    for which in range(2):
-        for half in range(HALVES):
-            send_own(which, half)
-
-    loads[0].wait()
+    send_quarter(0)
+
+    window = jnp.left_shift(jnp.int32(2), tp)
+    behind = lax.broadcasted_iota(jnp.int32, (rows, rows), 0) - lax.broadcasted_iota(
+        jnp.int32, (rows, rows), 1
+    )
+    for copy in prior:
+        copy.wait_recv()
+    for which in (0, 5, 6):
+        loads[which].wait()
+
+    def send_partial(owner):
+        return remote(partial.at[owner], tiles.at[tp], tile_send, tile_recv, (sp, owner))
+
+    earlier = None
+    for step in (2, 1, 3, 0):
+        owner = (tp + step) % tp_count
+        here = jnp.broadcast_to(docs[owner + 1].astype(jnp.float32), (rows, rows))
+        before = jnp.broadcast_to(docs[owner].astype(jnp.float32), (rows, rows))
+        mine = here.T
+        reach = jnp.where(sp * tp_count + owner > 0, window, 0)
+        near = jnp.where((behind >= 0) & (behind < window) & (here == mine), 1.0, 0.0)
+        far = jnp.where((behind + rows < reach) & (before == mine), 1.0, 0.0)
+        counts = jnp.sum(near + far, axis=1, keepdims=True)
+        current = pool_rows[owner + 1]
+        running = jnp.dot(
+            near.astype(jnp.bfloat16), current, preferred_element_type=jnp.float32
+        ) + jnp.dot(
+            far.astype(jnp.bfloat16), pool_rows[owner], preferred_element_type=jnp.float32
+        )
+        pooled = (running / counts - current.astype(jnp.float32)).astype(jnp.bfloat16)
+        branch = (
+            jnp.dot(pooled, pool_map[...], preferred_element_type=jnp.float32) * scale_ref[...]
+        ).astype(jnp.bfloat16)
+        block = jnp.dot(branch, project[...], preferred_element_type=jnp.float32).astype(
+            jnp.bfloat16
+        )
+        if step:
+            partial[owner] = block
+        else:
+            tiles[tp] = block
+        if earlier is not None:
+            send_partial(earlier).start()
+        earlier = owner
+    send_quarter(1)
+    send_own(0, 1)
+    send_own(1, 0)
+    send_own(1, 1)
+
     loads[1].wait()
     summed_tiles = remote(
         tiles.at[pl.ds(0, tp_count - 1)],
@@ -234,8 +310,8 @@
         fwd_copy(which, 0, 1).start()
         wait_own(which, 0, 0)
         wait_own(which, 1, 1)
-    for half in range(HALVES):
-        send_own(2, half)
+    send_own(2, 0)
+    send_own(2, 1)
 
     all_rows = remote(
         packed.at[pl.ds(0, (experts - 1) * capacity)],
@@ -273,12 +349,15 @@
     run_hidden(across)
 
     row_step = 128
-    for half in range(HALVES):
+    lines = capacity * col_blocks
+    for q in range(CHUNKS):
         for way in range(2):
-            wait_own(2, half, way)
-            fwd_copy(2, half, way).start()
+            wait_own(2, q, way)
+            fwd_copy(2, q, way).start()
+        if q + 2 < CHUNKS:
+            send_own(2, q + 2)
         for way in range(2):
-            fwd_copy(2, half, way).wait_recv()
+            fwd_copy(2, q, way).wait_recv()
 
         @pl.loop(0, slots // row_step)
         def _(i):
@@ -287,7 +366,7 @@
             for block in range(tp_count):
                 piece = jnp.dot(
                     hidden[block, at, :],
-                    all_down[block, :, half * columns : (half + 1) * columns],
+                    all_down[block, :, q * columns : (q + 1) * columns],
                     preferred_element_type=jnp.float32,
                 )
                 total = total + piece.astype(jnp.bfloat16).astype(jnp.float32)
@@ -296,11 +375,9 @@
                     total[:, c * LANES : (c + 1) * LANES]
                 )
 
-        lines = capacity * col_blocks
-
         @pl.loop(0, experts)
         def _(j):
-            sending[half, j] = shaped[pl.ds(pl.multiple_of(j * lines, lines), lines), :].astype(
+            sending[q, j] = shaped[pl.ds(pl.multiple_of(j * lines, lines), lines), :].astype(
                 jnp.bfloat16
             )
 
@@ -308,58 +385,70 @@
         def _(step):
             peer = (sp + step) % experts
             remote(
-                sending.at[half, peer],
-                returned.at[half, sp],
-                out_send.at[half],
-                out_recv.at[half],
+                sending.at[q, peer],
+                returned.at[q, sp],
+                out_send.at[q],
+                out_recv.at[q],
                 (peer, tp),
             ).start()
 
-        returned[half, sp] = sending[half, sp]
-
-    def all_out(half):
+        returned[q, sp] = sending[q, sp]
+
+    def all_out(q):
         return remote(
-            sending.at[half, pl.ds(0, experts - 1)],
-            returned.at[half, pl.ds(0, experts - 1)],
-            out_send.at[half],
-            out_recv.at[half],
+            sending.at[q, pl.ds(0, experts - 1)],
+            returned.at[q, pl.ds(0, experts - 1)],
+            out_send.at[q],
+            out_recv.at[q],
             (sp, above),
         )
 
-    for half in range(HALVES):
-        all_out(half).wait_recv()
+    line = lax.broadcasted_iota(jnp.int32, (LINES, LANES), 0)
+    for q in range(CHUNKS):
+        all_out(q).wait_recv()
+        pairs = lines // LINES
 
         @pl.loop(0, experts)
         def _(j):
-            picked_from[pl.ds(j * capacity, capacity)] = (
-                returned[half, j].astype(jnp.float32).reshape(capacity, col_blocks, LANES)
+            picked_from[pl.ds(j * pairs, pairs)] = (
+                returned[q, j].astype(jnp.float32).reshape(pairs, LINES, LANES)
             )
+
+        def picked(slot):
+            tile = picked_from[slot // 2]
+            return jnp.where(slot % 2 == q % 2, tile, pltpu.roll(tile, col_blocks, 0))
 
         @pl.loop(0, rows, unroll=4)
         def _(t):
-            combined[pl.ds(pl.multiple_of(t * col_blocks, col_blocks), col_blocks), :] = (
-                weight_ref[2 * t] * picked_from[slot_ref[2 * t]]
-                + weight_ref[2 * t + 1] * picked_from[slot_ref[2 * t + 1]]
+            both = weight_ref[2 * t] * picked(slot_ref[2 * t]) + weight_ref[2 * t + 1] * picked(
+                slot_ref[2 * t + 1]
             )
+            at = pl.ds(pl.multiple_of(t * LINES, LINES), LINES)
+            if q % 2:
+                both = jnp.where(line < col_blocks, combined[at, :], both)
+            combined[at, :] = both
 
         for c in range(col_blocks):
-            at = slice(half * columns + c * LANES, half * columns + (c + 1) * LANES)
+            at = slice(q * columns + c * LANES, q * columns + (c + 1) * LANES)
             out_ref[:, at] = (
-                mixed[:, at] + combined[pl.ds(c, rows, stride=col_blocks), :]
+                mixed[:, at]
+                + combined[pl.ds((q % 2) * col_blocks + c, rows, stride=LINES), :]
             ).astype(jnp.bfloat16)
 
+    for copy in prior:
+        copy.wait_send()
     summed_tiles.wait_send()
     all_rows.wait_send()
-    for half in range(HALVES):
-        all_out(half).wait_send()
-        for way in range(2):
-            for which in range(3):
+    for q in range(CHUNKS):
+        all_out(q).wait_send()
+    for way in range(2):
+        for q in range(CHUNKS):
+            own_copy(2, q, way).wait_send()
+            fwd_copy(2, q, way).wait_send()
+        for which in range(2):
+            for half in range(HALVES):
                 own_copy(which, half, way).wait_send()
-    for way in range(2):
-        for half in range(HALVES):
-            fwd_copy(2, half, way).wait_send()
-        fwd_copy(0, 0, way).wait_send()
-        fwd_copy(1, 0, way).wait_send()
+            fwd_copy(which, 0, way).wait_send()
 
 
 def per_device(
@@ -384,39 +473,13 @@
     quarter = row_count // tp_count
     capacity = max(2, 3 * top_count * quarter // (2 * expert_count))
     ff_part = expert_gate.shape[2]
-    reach_rows = SPAN - 1
-    tail_rows = (
-        pool_in[row_count - reach_rows :],
-        doc_ids[row_count - reach_rows :].astype(jnp.bfloat16),
-    )
-    prior_rows, prior_docs = passed_along((tail_rows[0], tail_rows[1]), "sp", 1)
-    extended = jnp.concatenate([prior_rows, pool_in], axis=0).astype(jnp.float32)
-    extended_docs = jnp.concatenate([prior_docs.astype(jnp.float32), doc_ids.astype(jnp.float32)])
-    own_docs = doc_ids.astype(jnp.float32)
-    window = jnp.left_shift(jnp.int32(2), lax.axis_index("tp"))
-    positions = lax.axis_index("sp") * row_count + jnp.arange(row_count, dtype=jnp.int32)
-    running = jnp.zeros(pool_in.shape, jnp.float32)
-    counts = jnp.zeros((row_count,), jnp.float32)
-    for offset in range(reach_rows + 1):
-        begin_row = reach_rows - offset
-        piece_rows = extended[begin_row : begin_row + row_count]
-        piece_docs = extended_docs[begin_row : begin_row + row_count]
-        in_window = (offset < window) & (positions - offset >= 0) & (piece_docs == own_docs)
-        running = running + jnp.where(in_window[:, None], piece_rows, 0.0)
-        counts = counts + in_window.astype(jnp.float32)
-    pooled = (running / counts[:, None] - pool_in.astype(jnp.float32)).astype(jnp.bfloat16)
-    branch = (jnp.dot(pooled, pool_map[0], preferred_element_type=jnp.float32) * pool_scale).astype(
-        jnp.bfloat16
-    )
-    partial = jnp.dot(branch, out_weight, preferred_element_type=jnp.float32).astype(jnp.bfloat16)
-    partial = partial.reshape(tp_count, quarter, model_width)
-
     own_routes = lax.dynamic_slice_in_dim(routes, lax.axis_index("tp") * quarter, quarter, 0)
     own_slots, own_sources = slot_table(own_routes, expert_count, capacity, top_count)
 
     slots = expert_count * capacity
     blocks = model_width // LANES
-    half_blocks = blocks // HALVES
+    chunk_blocks = blocks // CHUNKS
+    pool_width, group_out = pool_map.shape[1:]
     bf16, f32 = jnp.bfloat16, jnp.float32
     vmem, dma = pltpu.VMEM, pltpu.SemaphoreType.DMA
     smem_spec = pl.BlockSpec(memory_space=pltpu.SMEM)
@@ -425,9 +488,20 @@
     return pl.pallas_call(
         functools.partial(layer_kernel, expert_count, capacity, tp_count),
         out_shape=jax.ShapeDtypeStruct((quarter, model_width), bf16),
-        in_specs=[smem_spec] * 3 + [any_spec] * 2 + [vmem_spec] + [any_spec] * 3,
+        in_specs=[smem_spec] * 3
+        + [vmem_spec]
+        + [any_spec] * 2
+        + [vmem_spec]
+        + [any_spec] * 2
+        + [vmem_spec]
+        + [any_spec] * 3,
         out_specs=vmem_spec,
         scratch_shapes=[
+            vmem((tp_count + 1, quarter, pool_width), bf16),
+            vmem((tp_count + 1, 1, quarter), jnp.int32),
+            vmem((pool_width, group_out), bf16),
+            vmem((group_out, model_width), bf16),
+            vmem((tp_count, quarter, model_width), bf16),
             vmem((tp_count, quarter, model_width), bf16),
             vmem((quarter, model_width), bf16),
             vmem((quarter, model_width), f32),
@@ -441,22 +515,24 @@
             vmem((tp_count, model_width, ff_part), bf16),
             vmem((tp_count, ff_part, model_width), bf16),
             vmem((tp_count, slots, ff_part), bf16),
-            vmem((slots * half_blocks, LANES), f32),
-            vmem((HALVES, expert_count, capacity * half_blocks, LANES), bf16),
-            vmem((HALVES, expert_count, capacity * half_blocks, LANES), bf16),
-            vmem((slots, half_blocks, LANES), f32),
-            vmem((quarter * half_blocks, LANES), f32),
-            dma((5,)),
+            vmem((slots * chunk_blocks, LANES), f32),
+            vmem((CHUNKS, expert_count, capacity * chunk_blocks, LANES), bf16),
+            vmem((CHUNKS, expert_count, capacity * chunk_blocks, LANES), bf16),
+            vmem((slots * chunk_blocks // LINES, LINES, LANES), f32),
+            vmem((quarter * LINES, LANES), f32),
+            dma((7,)),
+            dma((2,)),
+            dma((2,)),
             dma,
             dma,
             dma,
             dma,
-            dma((HALVES,)),
-            dma((HALVES,)),
-            dma((2, 3, HALVES)),
-            dma((2, 3, HALVES)),
-            dma((2, 3, HALVES)),
-            dma((2, 3, HALVES)),
+            dma((CHUNKS,)),
+            dma((CHUNKS,)),
+            dma((2, 3, CHUNKS)),
+            dma((2, 3, CHUNKS)),
+            dma((2, 3, CHUNKS)),
+            dma((2, 3, CHUNKS)),
         ],
         compiler_params=pltpu.CompilerParams(
             collective_id=0, has_side_effects=True, vmem_limit_bytes=56 * 1024 * 1024
@@ -465,7 +541,11 @@
         own_sources,
         own_slots,
         route_weight.reshape(-1),
-        partial,
+        doc_ids.reshape(tp_count, 1, quarter),
+        pool_in.reshape(tp_count, quarter, pool_width),
+        pool_map[0],
+        pool_scale.reshape(1, -1),
+        out_weight,
         stream,
         norm_gain.reshape(1, -1),
         expert_gate[0],

time: 195 us -> 168 us (0.86)
  Pallas kernels: 173 us -> 162 us
  starting transfers between devices: 6.39 us -> 0 us
  matrix products: 5.39 us -> 0 us
  other arithmetic: 4.24 us -> 1.51 us
    pallas_call x1, Pallas kernels: 173 us -> 162 us  [per_device(): pl.pallas_call(functools.partial(layer_kernel, expert_count, capacity, tp...]
    ppermute x2 -> x0, starting transfers between devices: 6.39 us -> none  [passed_along(): return lax.ppermute(value, axis, pairs)]
    dot_general x1 -> x0, matrix products: 5.39 us -> none  [per_device(): jnp.dot(branch, out_weight, preferred_element_type=jnp.float32)]
  transfers between devices with their start and end apart: 2 -> 0, of which waited for: 0 -> 0; matrix products, arithmetic and copies ran while one was open for 3% -> 0% of each run, Pallas kernels for 0% -> 0%
where the time goes in v3:
time: 168 us
  Pallas kernels  162 us (96%)
  local copies, waits for them, and re-layouts  4.63 us (3%)
    pallas_call x1, Pallas kernels, per_device(): pl.pallas_call(functools.partial(layer_kernel, expert_count, capacity, tp...  162 us

profile of v3, /device:TPU:1, one launch (start us, length us, event | category | flops | bytes accessed | tf_op | source)
XLA Modules:
  0.0 168.2 jit_solution(4097430175859272359)
XLA Ops:
  0.0 0.0 copy-start
  0.0 0.7 copy-done
  0.7 0.1 copy.17
  0.8 0.1 reshape.43
  0.9 0.1 eq.39
  1.1 0.6 reduce-window.6
  1.7 0.2 slice_reduce_fusion
  1.9 0.1 fusion.2
  2.1 0.0 copy-start.1
  2.1 0.1 select_reduce_fusion
  2.2 0.6 add_select_fusion.source_ref
  2.8 0.8 copy.20
  3.6 0.7 reshape.45.weight_ref
  4.3 0.0 copy-done.1
  4.3 162.1 %shard_map.118 = bf16[128,2048]{1,0:T(8,128)(2,1)} custom-call(s32[384]{0:T(512)} %add_select_fusion.source_ref, s32[256]{0:T(256)} %copy-done.1, f32[256]{0:T(256)} %reshape.45.weight_ref, s32[4,1,128]{2,1,0:T(1,128)} %bitcast.33, bf16[4,128,256]{2,1,0:T(8,128)(2,1)} %bitcast.30, bf16[256,512]{1,0:T(8,128)(2,1)} %bitcast.31, f32[1,512]{1,0:T(1,128)} %bitcast.34, ...), custom_call_target="tpu_custom_call" | custom-call | tf_op jit(solution)/shard_map/pallas_call | solution.py:488
  166.4 1.9 %copy.24 = bf16[128,2048]{1,0:T(8,128)(2,1)} copy(bf16[128,2048]{1,0:T(8,128)(2,1)} %shard_map.118) | data formatting | bytes 1048576
  (5 shorter events, 0.1 us)
Async XLA Ops:
  0.0 0.7 copy-start
  2.1 2.2 %copy-start.1 = (s32[256]{0:T(256)}, s32[256]{0:T(256)S(1)}, u32[]{:S(2)}) copy-start(s32[256]{0:T(256)S(1)} %multiply_add_fusion.slot_ref) | copy-start | bytes 3076

commit v4 on v3

--- a/solution.py
+++ b/solution.py
@@ -13,29 +13,16 @@
 HALVES = 2
 CHUNKS = 4
 LINES = 8
-
-
-def slot_table(route_block, expert_count, capacity, top_count):
-    flattened = route_block.reshape(-1)
-    one_hot = (flattened[:, None] == jnp.arange(expert_count, dtype=jnp.int32)[None, :]).astype(
-        jnp.int32
-    )
-    ranking = jnp.sum((jnp.cumsum(one_hot, axis=0) - one_hot) * one_hot, axis=1)
-    target_slot = flattened * capacity + ranking
-    matches = target_slot[None, :] == jnp.arange(expert_count * capacity, dtype=jnp.int32)[:, None]
-    sources = jnp.sum(
-        jnp.where(matches, jnp.arange(flattened.shape[0], dtype=jnp.int32)[None, :], 0), axis=1
-    )
-    return (target_slot, sources // top_count)
+GRID = (8, 4, 2)
 
 
 def layer_kernel(
     experts,
     capacity,
     tp_count,
-    source_ref,
-    slot_ref,
+    grid,
     weight_ref,
+    routes_ref,
     docs_ref,
     pool_hbm,
     map_hbm,
@@ -52,6 +39,7 @@
     pool_map,
     project,
     partial,
+    relayed,
     tiles,
     stream_v,
     mixed,
@@ -70,9 +58,15 @@
     returned,
     picked_from,
     combined,
+    table,
+    table_s,
     local_sem,
+    heard,
+    table_sem,
     prior_send,
     prior_recv,
+    relay_send,
+    relay_recv,
     tile_send,
     tile_recv,
     row_send,
@@ -105,17 +99,40 @@
             device_id_type=MESH,
         )
 
+    deep, wide_x, cores = grid
+    core = sp % cores
+    x_at = (sp // cores) % wide_x
+    z_at = sp // (cores * wide_x)
+
+    def plane(dz, dx, dc):
+        return (
+            (((z_at + dz) % deep) * wide_x + (x_at + dx) % wide_x) * cores + (core + dc) % cores,
+            tp,
+        )
+
     barrier = pltpu.get_barrier_semaphore()
-    for step in range(1, tp_count):
-        pl.semaphore_signal(
-            barrier, inc=1, device_id=(sp, (tp + step) % tp_count), device_id_type=MESH
-        )
-
-    @pl.loop(1, experts)
-    def _(step):
-        pl.semaphore_signal(
-            barrier, inc=1, device_id=((sp + step) % experts, tp), device_id_type=MESH
-        )
+    near_devices = [(sp, (tp + step) % tp_count) for step in range(1, tp_count)]
+    near_devices += [plane(0, 0, 1), plane(1, 0, 0), plane(deep - 1, 0, 0)]
+    near_devices += [plane(0, dx, 0) for dx in range(1, wide_x)]
+    near_devices += [((sp + 1) % experts, tp), ((sp + experts - 1) % experts, tp)]
+    for device in near_devices:
+        pl.semaphore_signal(barrier, inc=1, device_id=device, device_id_type=MESH)
+
+    rounds = [
+        [plane(0, 0, 1)],
+        [plane(1, 0, 0), plane(deep - 1, 0, 0)],
+        [plane(1, 0, 0), plane(deep - 1, 0, 0)],
+        [plane(2, 0, 0), plane(deep - 2, 0, 0)],
+    ]
+
+    def tell(number):
+        for device in rounds[number]:
+            pl.semaphore_signal(
+                heard.at[number], inc=1, device_id=device, device_id_type=MESH
+            )
+
+    def hear(number):
+        pl.semaphore_wait(heard.at[number], len(rounds[number]))
 
     loads = [
         pltpu.make_async_copy(pool_hbm, pool_rows.at[pl.ds(1, tp_count)], local_sem.at[0]),
@@ -129,7 +146,8 @@
     for which in (0, 5, 6, 1, 2, 3, 4):
         loads[which].start()
     docs[1 : tp_count + 1] = docs_ref[...]
-    pl.semaphore_wait(barrier, experts - 1 + tp_count - 1)
+    pl.semaphore_wait(barrier, len(near_devices))
+    tell(0)
 
     following = ((sp + 1) % experts, tp)
     prior = [
@@ -203,6 +221,26 @@
 
     send_quarter(0)
 
+    def make_table():
+        down_rows = lax.broadcasted_iota(jnp.int32, (rows, rows), 0)
+        along = lax.broadcasted_iota(jnp.int32, (rows, rows), 1)
+        at = pl.ds(pl.multiple_of(tp * rows, rows), rows)
+        named = [jnp.broadcast_to(routes_ref[k : k + 1, at], (rows, rows)) for k in range(2)]
+        turned = [value.T for value in named]
+        found = []
+        for k in range(2):
+            same = jnp.where(turned[0] == named[k], 1, 0) + jnp.where(turned[1] == named[k], 1, 0)
+            rank = jnp.sum(jnp.where(down_rows < along, same, 0), axis=0, keepdims=True)
+            found.append(named[k][0:1, :] * capacity + rank)
+            table[k : k + 1, :] = found[k]
+        spread = [jnp.broadcast_to(value, (rows, rows)).T for value in found]
+        for m in range(slots // LANES):
+            held = (spread[0] == along + m * LANES) | (spread[1] == along + m * LANES)
+            table[2 + m : 3 + m, :] = jnp.sum(
+                jnp.where(held, down_rows, 0), axis=0, keepdims=True
+            )
+        pltpu.make_async_copy(table, table_s, table_sem).start()
+
     window = jnp.left_shift(jnp.int32(2), tp)
     behind = lax.broadcasted_iota(jnp.int32, (rows, rows), 0) - lax.broadcasted_iota(
         jnp.int32, (rows, rows), 1
@@ -212,10 +250,28 @@
     for which in (0, 5, 6):
         loads[which].wait()
 
-    def send_partial(owner):
-        return remote(partial.at[owner], tiles.at[tp], tile_send, tile_recv, (sp, owner))
-
-    earlier = None
+    half_rows = rows // 2
+
+    def relay_copy(way):
+        return remote(
+            partial.at[across, pl.ds(way * half_rows, half_rows)],
+            relayed.at[way],
+            relay_send.at[way],
+            relay_recv.at[way],
+            (sp, above if way == 0 else below),
+        )
+
+    def tile_copy(way, half):
+        owner = above if way == 0 else below
+        at = pl.ds(half * half_rows, half_rows)
+        return remote(
+            partial.at[owner, at],
+            tiles.at[way, at],
+            tile_send.at[way, half],
+            tile_recv.at[way, half],
+            (sp, owner),
+        )
+
     for step in (2, 1, 3, 0):
         owner = (tp + step) % tp_count
         here = jnp.broadcast_to(docs[owner + 1].astype(jnp.float32), (rows, rows))
@@ -241,24 +297,37 @@
         if step:
             partial[owner] = block
         else:
-            tiles[tp] = block
-        if earlier is not None:
-            send_partial(earlier).start()
-        earlier = owner
+            tiles[2] = block
+        if step != 2:
+            number = (1, 3, 0).index(step)
+            hear(number)
+            tell(number + 1)
+        if step == 1:
+            relay_copy(0).start()
+            relay_copy(1).start()
+        elif step == 3:
+            tile_copy(0, 1).start()
+        elif step == 0:
+            tile_copy(1, 0).start()
+    for way in range(2):
+        owner = above if way == 0 else below
+        at = pl.ds(way * half_rows, half_rows)
+        relay_copy(way).wait_recv()
+        partial[owner, at, :] = (
+            partial[owner, at, :].astype(jnp.float32) + relayed[way].astype(jnp.float32)
+        ).astype(jnp.bfloat16)
+    make_table()
+    for way in range(2):
+        tile_copy(way, way).start()
     send_quarter(1)
     send_own(0, 1)
     send_own(1, 0)
     send_own(1, 1)
 
     loads[1].wait()
-    summed_tiles = remote(
-        tiles.at[pl.ds(0, tp_count - 1)],
-        tiles.at[pl.ds(0, tp_count - 1)],
-        tile_send,
-        tile_recv,
-        (sp, above),
-    )
-    summed_tiles.wait_recv()
+    for way in range(2):
+        for half in range(2):
+            tile_copy(way, half).wait_recv()
 
     step_rows = 16
 
@@ -266,7 +335,7 @@
     def _(i):
         at = pl.ds(pl.multiple_of(i * step_rows, step_rows), step_rows)
         total = tiles[0, at, :].astype(jnp.float32)
-        for k in range(1, tp_count):
+        for k in range(1, 3):
             total = total + tiles[k, at, :].astype(jnp.float32)
         here = (stream_v[at, :].astype(jnp.float32) + total).astype(jnp.bfloat16)
         here = here.astype(jnp.float32)
@@ -284,9 +353,12 @@
             jnp.bfloat16
         )
 
+    hear(3)
+    pltpu.make_async_copy(table, table_s, table_sem).wait()
+
     @pl.loop(0, slots, unroll=4)
     def _(s):
-        packed[s] = rounded[source_ref[s]]
+        packed[s] = rounded[table_s[2 + s // LANES, s % LANES]]
 
     @pl.loop(1, experts)
     def _(step):
@@ -420,8 +492,8 @@
 
         @pl.loop(0, rows, unroll=4)
         def _(t):
-            both = weight_ref[2 * t] * picked(slot_ref[2 * t]) + weight_ref[2 * t + 1] * picked(
-                slot_ref[2 * t + 1]
+            both = weight_ref[0, t] * picked(table_s[0, t]) + weight_ref[1, t] * picked(
+                table_s[1, t]
             )
             at = pl.ds(pl.multiple_of(t * LINES, LINES), LINES)
             if q % 2:
@@ -437,7 +509,10 @@
 
     for copy in prior:
         copy.wait_send()
-    summed_tiles.wait_send()
+    for way in range(2):
+        relay_copy(way).wait_send()
+        for half in range(2):
+            tile_copy(way, half).wait_send()
     all_rows.wait_send()
     for q in range(CHUNKS):
         all_out(q).wait_send()
@@ -473,9 +548,6 @@
     quarter = row_count // tp_count
     capacity = max(2, 3 * top_count * quarter // (2 * expert_count))
     ff_part = expert_gate.shape[2]
-    own_routes = lax.dynamic_slice_in_dim(routes, lax.axis_index("tp") * quarter, quarter, 0)
-    own_slots, own_sources = slot_table(own_routes, expert_count, capacity, top_count)
-
     slots = expert_count * capacity
     blocks = model_width // LANES
     chunk_blocks = blocks // CHUNKS
@@ -486,10 +558,10 @@
     any_spec = pl.BlockSpec(memory_space=pl.ANY)
     vmem_spec = pl.BlockSpec(memory_space=pltpu.VMEM)
     return pl.pallas_call(
-        functools.partial(layer_kernel, expert_count, capacity, tp_count),
+        functools.partial(layer_kernel, expert_count, capacity, tp_count, GRID),
         out_shape=jax.ShapeDtypeStruct((quarter, model_width), bf16),
-        in_specs=[smem_spec] * 3
-        + [vmem_spec]
+        in_specs=[smem_spec]
+        + [vmem_spec] * 2
         + [any_spec] * 2
         + [vmem_spec]
         + [any_spec] * 2
@@ -502,7 +574,8 @@
             vmem((pool_width, group_out), bf16),
             vmem((group_out, model_width), bf16),
             vmem((tp_count, quarter, model_width), bf16),
-            vmem((tp_count, quarter, model_width), bf16),
+            vmem((2, quarter // 2, model_width), bf16),
+            vmem((3, quarter, model_width), bf16),
             vmem((quarter, model_width), bf16),
             vmem((quarter, model_width), f32),
             vmem((quarter * blocks, LANES), f32),
@@ -520,11 +593,17 @@
             vmem((CHUNKS, expert_count, capacity * chunk_blocks, LANES), bf16),
             vmem((slots * chunk_blocks // LINES, LINES, LANES), f32),
             vmem((quarter * LINES, LANES), f32),
+            vmem((8, LANES), jnp.int32),
+            pltpu.SMEM((8, LANES), jnp.int32),
             dma((7,)),
+            pltpu.SemaphoreType.REGULAR((4,)),
+            dma,
             dma((2,)),
             dma((2,)),
-            dma,
-            dma,
+            dma((2,)),
+            dma((2,)),
+            dma((2, 2)),
+            dma((2, 2)),
             dma,
             dma,
             dma((CHUNKS,)),
@@ -538,9 +617,8 @@
             collective_id=0, has_side_effects=True, vmem_limit_bytes=56 * 1024 * 1024
         ),
     )(
-        own_sources,
-        own_slots,
-        route_weight.reshape(-1),
+        route_weight.T,
+        routes.T,
         doc_ids.reshape(tp_count, 1, quarter),
         pool_in.reshape(tp_count, quarter, pool_width),
         pool_map[0],

time: 168 us -> 157 us (0.935)
  Pallas kernels: 162 us -> 155 us
  local copies, waits for them, and re-layouts: 4.63 us -> 1.88 us
    pallas_call x1, Pallas kernels: 162 us -> 155 us  [per_device(): pl.pallas_call(functools.partial(layer_kernel, expert_count, capacity, tp...]
where the time goes in v4:
time: 157 us
  Pallas kernels  155 us (99%)
  local copies, waits for them, and re-layouts  1.88 us (1%)
    pallas_call x1, Pallas kernels, per_device(): pl.pallas_call(functools.partial(layer_kernel, expert_count, capacity, tp...  155 us

profile of v4, /device:TPU:1, one launch (start us, length us, event | category | flops | bytes accessed | tf_op | source)
XLA Modules:
  0.0 156.8 jit_solution(15837479585687479457)
XLA Ops:
  0.0 154.9 %shard_map.118 = bf16[128,2048]{1,0:T(8,128)(2,1)} custom-call(f32[2,128]{1,0:T(2,128)} %bitcast.19, s32[2,512]{1,0:T(2,128)} %bitcast.16, s32[4,1,128]{2,1,0:T(1,128)} %bitcast.17, bf16[4,128,256]{2,1,0:T(8,128)(2,1)} %bitcast.13, bf16[256,512]{1,0:T(8,128)(2,1)} %bitcast.14, f32[1,512]{1,0:T(1,128)} %bitcast.18, bf16[512,2048]{1,0:T(8,128)(2,1)} %project_hbm.1, ...), custom_call_target="tpu_custom_call" | custom-call | tf_op jit(solution)/shard_map/pallas_call | solution.py:560
  155.0 1.9 %copy.14 = bf16[128,2048]{1,0:T(8,128)(2,1)} copy(bf16[128,2048]{1,0:T(8,128)(2,1)} %shard_map.118) | data formatting | bytes 1048576

commit v5 on v4

--- a/solution.py
+++ b/solution.py
@@ -360,7 +360,7 @@
     def _(s):
         packed[s] = rounded[table_s[2 + s // LANES, s % LANES]]
 
-    @pl.loop(1, experts)
+    @pl.loop(1, experts, unroll=7)
     def _(step):
         peer = (sp + step) % experts
         remote(
@@ -422,12 +422,18 @@
 
     row_step = 128
     lines = capacity * col_blocks
-    for q in range(CHUNKS):
+
+    def pass_down(q):
         for way in range(2):
             wait_own(2, q, way)
             fwd_copy(2, q, way).start()
         if q + 2 < CHUNKS:
             send_own(2, q + 2)
+
+    pass_down(0)
+    for q in range(CHUNKS):
+        if q + 1 < CHUNKS:
+            pass_down(q + 1)
         for way in range(2):
             fwd_copy(2, q, way).wait_recv()
 
@@ -447,13 +453,13 @@
                     total[:, c * LANES : (c + 1) * LANES]
                 )
 
-        @pl.loop(0, experts)
+        @pl.loop(0, experts, unroll=8)
         def _(j):
             sending[q, j] = shaped[pl.ds(pl.multiple_of(j * lines, lines), lines), :].astype(
                 jnp.bfloat16
             )
 
-        @pl.loop(1, experts)
+        @pl.loop(1, experts, unroll=7)
         def _(step):
             peer = (sp + step) % experts
             remote(
@@ -480,7 +486,7 @@
         all_out(q).wait_recv()
         pairs = lines // LINES
 
-        @pl.loop(0, experts)
+        @pl.loop(0, experts, unroll=8)
         def _(j):
             picked_from[pl.ds(j * pairs, pairs)] = (
                 returned[q, j].astype(jnp.float32).reshape(pairs, LINES, LANES)
@@ -490,7 +496,7 @@
             tile = picked_from[slot // 2]
             return jnp.where(slot % 2 == q % 2, tile, pltpu.roll(tile, col_blocks, 0))
 
-        @pl.loop(0, rows, unroll=4)
+        @pl.loop(0, rows, unroll=16)
         def _(t):
             both = weight_ref[0, t] * picked(table_s[0, t]) + weight_ref[1, t] * picked(
                 table_s[1, t]
@@ -559,7 +565,7 @@
     vmem_spec = pl.BlockSpec(memory_space=pltpu.VMEM)
     return pl.pallas_call(
         functools.partial(layer_kernel, expert_count, capacity, tp_count, GRID),
-        out_shape=jax.ShapeDtypeStruct((quarter, model_width), bf16),
+        out_shape=pltpu.VMEM((quarter, model_width), bf16),
         in_specs=[smem_spec]
         + [vmem_spec] * 2
         + [any_spec] * 2

time: 157 us -> 153 us (0.975)
  Pallas kernels: 155 us -> 152 us
    pallas_call x1, Pallas kernels: 155 us -> 152 us  [per_device(): pl.pallas_call(functools.partial(layer_kernel, expert_count, capacity, tp...]
where the time goes in v5:
time: 153 us
  Pallas kernels  152 us (99%)
    pallas_call x1, Pallas kernels, per_device(): pl.pallas_call(functools.partial(layer_kernel, expert_count, capacity, tp...  152 us

profile of v5, /device:TPU:1, one launch (start us, length us, event | category | flops | bytes accessed | tf_op | source)
XLA Modules:
  0.0 153.1 jit_solution(1612318867224219391)
XLA Ops:
  0.0 152.3 %shard_map.118 = bf16[128,2048]{1,0:T(8,128)(2,1)S(1)} custom-call(f32[2,128]{1,0:T(2,128)} %bitcast.19, s32[2,512]{1,0:T(2,128)} %bitcast.16, s32[4,1,128]{2,1,0:T(1,128)} %bitcast.17, bf16[4,128,256]{2,1,0:T(8,128)(2,1)} %bitcast.13, bf16[256,512]{1,0:T(8,128)(2,1)} %bitcast.14, f32[1,512]{1,0:T(1,128)} %bitcast.18, bf16[512,2048]{1,0:T(8,128)(2,1)} %project_hbm.1, ...), custom_call_target="tpu_custom_call" | custom-call | tf_op jit(solution)/shard_map/pallas_call | solution.py:566
  152.3 0.8 copy.14

commit v6 on v5

--- a/solution.py
+++ b/solution.py
@@ -58,6 +58,7 @@
     returned,
     picked_from,
     combined,
+    early,
     table,
     table_s,
     local_sem,
@@ -316,13 +317,13 @@
         partial[owner, at, :] = (
             partial[owner, at, :].astype(jnp.float32) + relayed[way].astype(jnp.float32)
         ).astype(jnp.bfloat16)
-    make_table()
     for way in range(2):
         tile_copy(way, way).start()
     send_quarter(1)
     send_own(0, 1)
     send_own(1, 0)
     send_own(1, 1)
+    make_table()
 
     loads[1].wait()
     for way in range(2):
@@ -434,20 +435,29 @@
     for q in range(CHUNKS):
         if q + 1 < CHUNKS:
             pass_down(q + 1)
-        for way in range(2):
-            fwd_copy(2, q, way).wait_recv()
-
-        @pl.loop(0, slots // row_step)
-        def _(i):
-            at = pl.ds(pl.multiple_of(i * row_step, row_step), row_step)
-            total = jnp.zeros((row_step, columns), jnp.float32)
-            for block in range(tp_count):
-                piece = jnp.dot(
+        def down_part(block, at):
+            return (
+                jnp.dot(
                     hidden[block, at, :],
                     all_down[block, :, q * columns : (q + 1) * columns],
                     preferred_element_type=jnp.float32,
                 )
-                total = total + piece.astype(jnp.bfloat16).astype(jnp.float32)
+                .astype(jnp.bfloat16)
+                .astype(jnp.float32)
+            )
+
+        @pl.loop(0, slots // row_step)
+        def _(i):
+            at = pl.ds(pl.multiple_of(i * row_step, row_step), row_step)
+            early[at, :] = down_part(tp, at) + down_part(below, at) + down_part(above, at)
+
+        for way in range(2):
+            fwd_copy(2, q, way).wait_recv()
+
+        @pl.loop(0, slots // row_step)
+        def _(i):
+            at = pl.ds(pl.multiple_of(i * row_step, row_step), row_step)
+            total = early[at, :] + down_part(across, at)
             for c in range(col_blocks):
                 shaped[pl.ds(i * (row_step * col_blocks) + c, row_step, stride=col_blocks), :] = (
                     total[:, c * LANES : (c + 1) * LANES]
@@ -599,6 +609,7 @@
             vmem((CHUNKS, expert_count, capacity * chunk_blocks, LANES), bf16),
             vmem((slots * chunk_blocks // LINES, LINES, LANES), f32),
             vmem((quarter * LINES, LANES), f32),
+            vmem((slots, model_width // CHUNKS), f32),
             vmem((8, LANES), jnp.int32),
             pltpu.SMEM((8, LANES), jnp.int32),
             dma((7,)),

time: 153 us -> 153 us (level)
  no operation moved by 1% of the time
where the time goes in v6:
time: 153 us
  Pallas kernels  152 us (99%)
    pallas_call x1, Pallas kernels, per_device(): pl.pallas_call(functools.partial(layer_kernel, expert_count, capacity, tp...  152 us

profile of v6, /device:TPU:1, one launch (start us, length us, event | category | flops | bytes accessed | tf_op | source)
XLA Modules:
  0.0 152.9 jit_solution(2145392579540126733)
XLA Ops:
  0.0 152.1 %shard_map.118 = bf16[128,2048]{1,0:T(8,128)(2,1)S(1)} custom-call(f32[2,128]{1,0:T(2,128)} %bitcast.19, s32[2,512]{1,0:T(2,128)} %bitcast.16, s32[4,1,128]{2,1,0:T(1,128)} %bitcast.17, bf16[4,128,256]{2,1,0:T(8,128)(2,1)} %bitcast.13, bf16[256,512]{1,0:T(8,128)(2,1)} %bitcast.14, f32[1,512]{1,0:T(1,128)} %bitcast.18, bf16[512,2048]{1,0:T(8,128)(2,1)} %project_hbm.1, ...), custom_call_target="tpu_custom_call" | custom-call | tf_op jit(solution)/shard_map/pallas_call | solution.py:576
  152.1 0.8 copy.14
